TPU v7x, 32 devices: a whole 2x2x4 slice. The times are simulated.
32 devices in a mesh: ep: 8 (over z, x), tp: 4 (over y, core).
Axes of the slice: x: 2, y: 2, z: 4, core: 2. Of those that a mesh axis runs over, the one named last changes fastest.
Arguments:
- memory_query_matrix: bfloat16 [4096, 1024], P('ep', 'tp'), may hold values from -0.59765625 to 2
- memory_key_matrix: bfloat16 [4096, 1024], P('ep', 'tp'), may hold values from -0.59765625 to 2
- memory_value_matrix: bfloat16 [4096, 1024], P('ep', 'tp'), may hold values from -6 to 6
- input_gate_logits: float32 [4, 4096], P('tp', 'ep'), may hold values from -6 to 260
- forget_gate_logits: float32 [4, 4096], P('tp', 'ep'), may hold values from -1 to 20
- forget_log_boosts: float32 [4, 4096], P('tp', 'ep'), may hold values from -0.7 to 0
- head_norm_scale: float32 [1024], P('tp'), may hold values from 0.1 to 1.9
- memory_output_matrix: bfloat16 [1024, 2048], replicated, may hold values from -0.1875 to 0.1875
- projection_norm_scale: float32 [2048], replicated, may hold values from 0.1 to 1.9
- second_batch_rows: bfloat16 [6144, 2048], P(('ep', 'tp')), may hold values from -6 to 6
- expert_prenorm_scale: float32 [2048], replicated, may hold values from 0.1 to 1.9
- selected_expert_index: int32 [6144, 2], P(('ep', 'tp')), may hold values from 0 to 7, all different within a row; in each aligned block of 192 rows (0 to 191, 192 to 383, ...) at most 96 rows name the same one
- group_route_probability: float32 [6144], P(('ep', 'tp')), may hold values from 0.2 to 1
- expert_choice_scores: float32 [6144, 2], P(('ep', 'tp')), may hold values from -6 to 6
- expert_gate_matrix: bfloat16 [8, 2048, 512], P('ep'), may hold values from -0.125 to 0.125
- expert_up_matrix: bfloat16 [8, 2048, 512], P('ep'), may hold values from -0.125 to 0.125
- expert_down_matrix: bfloat16 [8, 512, 2048], P('ep'), may hold values from -0.25 to 0.25
Outputs:
- mixed_rows: bfloat16 [4096, 2048], P(('ep', 'tp'))
- routed_rows: bfloat16 [6144, 2048], P(('ep', 'tp'))
Inputs may be any that keep to these rules, and one draw needn't show every extreme that they name: `selected_expert_index`: each row names 2 different experts; among the rows of one device no expert is named more than 96 times, and in some device one expert is named exactly that often.
All inputs are finite; a program needn't handle non-finite values.
Results may differ from a plain program's by a relative error of at most 0.013.
Values may be sent and summed in bfloat16 or wider, within the bound.
A program may use at most 128 MiB of HBM per device.

v0:
```python
import functools

import jax
import jax.numpy as jnp
from jax import lax
from jax.experimental import pallas as pl
from jax.experimental.pallas import tpu as pltpu
from jax.sharding import PartitionSpec as P

FLOOR = -1e30
EPS = 1e-06
MESH = pl.DeviceIdType.MESH
F32 = jnp.float32
BF16 = jnp.bfloat16


def rms(values, gain):
    squares = jnp.mean(values * values, axis=-1, keepdims=True)
    return values * lax.rsqrt(squares + EPS) * gain


def dot(a, b, dims=((1,), (0,)), precision=None):
    return lax.dot_general(a, b, (dims, ((), ())), preferred_element_type=F32, precision=precision)


def join(early, late):
    total_e, peak_e, mem_e, nor_e = early
    total_l, peak_l, mem_l, nor_l = late
    peak = jnp.maximum(total_l + peak_e, peak_l)
    fe = jnp.exp(total_l + peak_e - peak)
    fl = jnp.exp(peak_l - peak)
    return (total_e + total_l, peak, fe * mem_e + fl * mem_l, fe * nor_e + fl * nor_l)


def kernel(
    n, nt, cap,
    q_ref, k_ref, v_ref, ig_ref, fg_ref, fb_ref, hs_ref, wo_hbm, ps_ref,
    x_ref, es_ref, ids_ref, grp_ref, sc_ref, wg_hbm, wu_hbm, wd_hbm,
    mixed_ref, routed_ref,
    wg, wu, wd, wo, out, recv, ans, back, ffn, acc,
    cpair, spair, cgrp, sgrp, ent, head, pout, prec,
    wsem, d_ss, d_rs, a_ss, a_rs, c1s, c1r, s1s, s1r, c2s, c2r, s2s, s2r, p_ss, p_rs,
):
    me = lax.axis_index("ep")
    tp = lax.axis_index("tp")
    groups = n // 2
    grp = me // 2
    par = lax.rem(me, 2)
    partner = me + 1 - 2 * par
    tokens, width = x_ref.shape
    length, hd = q_ref.shape
    rows = mixed_ref.shape[0]

    barrier = pltpu.get_barrier_semaphore()

    def greet(i, c):
        pl.semaphore_signal(barrier, inc=1, device_id=(lax.rem(me + i, n), tp), device_id_type=MESH)
        return c

    lax.fori_loop(1, n, greet, 0)
    for j in range(1, nt):
        pl.semaphore_signal(barrier, inc=1, device_id=(me, lax.rem(tp + j, nt)), device_id_type=MESH)

    loads = [
        pltpu.make_async_copy(wg_hbm.at[0], wg, wsem.at[0]),
        pltpu.make_async_copy(wu_hbm.at[0], wu, wsem.at[1]),
        pltpu.make_async_copy(wd_hbm.at[0], wd, wsem.at[2]),
        pltpu.make_async_copy(wo_hbm.at[pl.ds(pl.multiple_of(tp * hd, hd), hd)], wo, wsem.at[3]),
    ]
    for load in loads:
        load.start()

    fg = fg_ref[...]
    lk = jnp.minimum(fg, 0.0) - jnp.log1p(jnp.exp(-jnp.abs(fg))) + fb_ref[...]
    rid = lax.broadcasted_iota(jnp.int32, (length, length), 0)
    cid = lax.broadcasted_iota(jnp.int32, (length, length), 1)
    upper = (rid <= cid).astype(F32)
    b_row = dot(jnp.broadcast_to(lk, (8, length)), upper, precision=lax.Precision.HIGHEST)[0:1]
    i_row = ig_ref[...]
    last = b_row[:, length - 1 : length]
    g_row = last - b_row + i_row
    m_loc = jnp.max(g_row, axis=-1, keepdims=True)
    which = lax.broadcasted_iota(jnp.int32, (128, length), 0)
    cols = jnp.where(which == 0, b_row, g_row).T
    b_col = cols[:, 0:1]
    g_col = cols[:, 1:2]
    kw = k_ref[...].astype(F32) * (jnp.exp(g_col - m_loc) * (hd**-0.5))
    c_loc = dot(kw.astype(BF16), v_ref[...], ((0,), (0,)))
    n_loc = jnp.sum(kw, axis=0, keepdims=True)
    stat_id = lax.broadcasted_iota(jnp.int32, (8, hd), 0)

    def stats(total, peak, nor):
        return jnp.where(stat_id == 0, nor, jnp.where(stat_id == 1, peak, total))

    cpair[par] = c_loc.astype(BF16)
    spair[par] = stats(last, m_loc, n_loc)

    pl.semaphore_wait(barrier, n - 1 + nt - 1)

    def pair_copies():
        return [
            pltpu.make_async_remote_copy(
                src_ref=cpair.at[par], dst_ref=cpair.at[par], send_sem=c1s, recv_sem=c1r,
                device_id=(partner, tp), device_id_type=MESH),
            pltpu.make_async_remote_copy(
                src_ref=spair.at[par], dst_ref=spair.at[par], send_sem=s1s, recv_sem=s1r,
                device_id=(partner, tp), device_id_type=MESH),
        ]

    for copy in pair_copies():
        copy.start()

    ffn[...] = rms(x_ref[...].astype(F32), es_ref[...]).astype(BF16)
    ids = ids_ref[...]
    first, second = ids[:, 0:1], ids[:, 1:2]
    lane_e = lax.broadcasted_iota(jnp.int32, (tokens, n), 1)
    named = ((lane_e == first) | (lane_e == second)).astype(F32)
    tr = lax.broadcasted_iota(jnp.int32, (tokens, tokens), 0)
    tc = lax.broadcasted_iota(jnp.int32, (tokens, tokens), 1)
    rank = dot((tc < tr).astype(BF16), named.astype(BF16))
    slot_a = first * cap + jnp.sum(jnp.where(lane_e == first, rank, 0.0), axis=1, keepdims=True).astype(jnp.int32)
    slot_b = second * cap + jnp.sum(jnp.where(lane_e == second, rank, 0.0), axis=1, keepdims=True).astype(jnp.int32)
    score = sc_ref[...]
    ex = jnp.exp(score - jnp.max(score, axis=-1, keepdims=True))
    route = grp_ref[...] * (ex / jnp.sum(ex, axis=-1, keepdims=True))
    rw_a, rw_b = route[:, 0:1], route[:, 1:2]
    lane_c = lax.broadcasted_iota(jnp.int32, (tokens, cap), 1)

    def pack(e):
        lane = lane_c + e * cap
        place = ((lane == slot_a) | (lane == slot_b)).astype(BF16)
        out[e] = dot(place, ffn[...], ((0,), (0,))).astype(BF16)

    def offset(i):
        return n // 2 + jnp.where(lax.rem(i, 2) == 0, i // 2, -((i + 1) // 2))

    def dispatch_copy(e):
        return pltpu.make_async_remote_copy(
            src_ref=out.at[e], dst_ref=recv.at[me], send_sem=d_ss.at[e], recv_sem=d_rs.at[me],
            device_id=(e, tp), device_id_type=MESH)

    def dispatch_arrival(s):
        return pltpu.make_async_remote_copy(
            src_ref=out.at[s], dst_ref=recv.at[s], send_sem=d_ss.at[s], recv_sem=d_rs.at[s],
            device_id=(s, tp), device_id_type=MESH)

    def answer_copy(s):
        return pltpu.make_async_remote_copy(
            src_ref=ans.at[s], dst_ref=back.at[me], send_sem=a_ss.at[s], recv_sem=a_rs.at[me],
            device_id=(s, tp), device_id_type=MESH)

    def answer_arrival(e):
        return pltpu.make_async_remote_copy(
            src_ref=ans.at[e], dst_ref=back.at[e], send_sem=a_ss.at[e], recv_sem=a_rs.at[e],
            device_id=(e, tp), device_id_type=MESH)

    for copy in pair_copies():
        copy.wait_send()
    def pair_arrival():
        return [
            pltpu.make_async_remote_copy(
                src_ref=cpair.at[1 - par], dst_ref=cpair.at[1 - par], send_sem=c1s, recv_sem=c1r,
                device_id=(partner, tp), device_id_type=MESH),
            pltpu.make_async_remote_copy(
                src_ref=spair.at[1 - par], dst_ref=spair.at[1 - par], send_sem=s1s, recv_sem=s1r,
                device_id=(partner, tp), device_id_type=MESH),
        ]

    for copy in pair_arrival():
        copy.wait_recv()

    def unpack(c, s):
        return (s[2:3], s[1:2], c.astype(F32), s[0:1])

    both = join(unpack(cpair[0], spair[0]), unpack(cpair[1], spair[1]))
    cgrp[grp] = both[2].astype(BF16)
    sgrp[grp] = stats(both[0], both[1], both[3])

    def group_copies(g):
        to = (g * 2 + par, tp)
        return [
            pltpu.make_async_remote_copy(
                src_ref=cgrp.at[grp], dst_ref=cgrp.at[grp], send_sem=c2s.at[g], recv_sem=c2r.at[grp],
                device_id=to, device_id_type=MESH),
            pltpu.make_async_remote_copy(
                src_ref=sgrp.at[grp], dst_ref=sgrp.at[grp], send_sem=s2s.at[g], recv_sem=s2r.at[grp],
                device_id=to, device_id_type=MESH),
        ]

    def group_arrivals(g):
        at = (g * 2 + par, tp)
        return [
            pltpu.make_async_remote_copy(
                src_ref=cgrp.at[g], dst_ref=cgrp.at[g], send_sem=c2s.at[g], recv_sem=c2r.at[g],
                device_id=at, device_id_type=MESH),
            pltpu.make_async_remote_copy(
                src_ref=sgrp.at[g], dst_ref=sgrp.at[g], send_sem=s2s.at[g], recv_sem=s2r.at[g],
                device_id=at, device_id_type=MESH),
        ]

    def send_group(g, c):
        for copy in group_copies(g):
            copy.start()
        return c

    lax.fori_loop(grp + 1, groups, send_group, 0)

    def send_tokens(i, c):
        e = lax.rem(me + offset(i), n)
        pack(e)
        dispatch_copy(e).start()
        return c

    lax.fori_loop(0, n - 1, send_tokens, 0)
    pack(me)
    for load in loads:
        load.wait()

    def expert(chosen):
        gate = dot(chosen, wg[...])
        up = dot(chosen, wu[...])
        hidden = (gate / (1.0 + jnp.exp(-gate)) * up).astype(BF16)
        return dot(hidden, wd[...]).astype(BF16)

    ans[me] = expert(out[me])

    ent[...] = jnp.zeros(ent.shape, F32)
    row1 = jnp.zeros((1, hd), F32)

    def enter(g, carry):
        total, peak, nor = carry
        for copy in group_arrivals(g):
            copy.wait_recv()
        total, peak, mem, nor = join((total, peak, ent[...], nor), unpack(cgrp[g], sgrp[g]))
        ent[...] = mem
        return total, peak, nor

    total, peak, nor = lax.fori_loop(0, grp, enter, (row1, row1 + FLOOR, row1))
    joined = join((total, peak, ent[...], nor), unpack(cpair[0], spair[0]))
    odd = par == 1
    m_in = jnp.where(odd, joined[1], peak)
    n_in = jnp.where(odd, joined[3], nor)
    c_in = jnp.where(odd, joined[2], ent[...])

    carried = b_col + m_in[:, 0:1]
    decay = jnp.where(cid <= rid, b_col - b_row + i_row, -jnp.inf)
    peaks = jnp.maximum(carried, jnp.max(decay, axis=-1, keepdims=True))
    across = jnp.exp(carried - peaks)
    scores = dot(q_ref[...], k_ref[...], ((1,), (1,))) * (hd**-0.5) * jnp.exp(decay - peaks)
    qf = q_ref[...].astype(F32)
    den = jnp.sum(scores, axis=-1, keepdims=True) + across * jnp.sum(qf * n_in, axis=-1, keepdims=True)
    num = dot(scores.astype(BF16), v_ref[...]) + across * dot(q_ref[...], c_in.astype(BF16))
    cell = num / jnp.maximum(jnp.abs(den), jnp.exp(-peaks))
    head[...] = (cell * hs_ref[...]).astype(BF16)

    def part_copy(j):
        return pltpu.make_async_remote_copy(
            src_ref=pout.at[j], dst_ref=prec.at[tp], send_sem=p_ss.at[j], recv_sem=p_rs.at[tp],
            device_id=(me, j), device_id_type=MESH)

    def part_arrival(j):
        return pltpu.make_async_remote_copy(
            src_ref=pout.at[j], dst_ref=prec.at[j], send_sem=p_ss.at[j], recv_sem=p_rs.at[j],
            device_id=(me, j), device_id_type=MESH)

    def project(j):
        pout[j] = dot(head[pl.ds(pl.multiple_of(j * rows, rows), rows), :], wo[...]).astype(BF16)

    def send_part(i, c):
        j = lax.rem(tp + i, nt)
        project(j)
        part_copy(j).start()
        return c

    lax.fori_loop(1, nt, send_part, 0)
    project(tp)

    def serve(i, c):
        s = lax.rem(me - offset(i) + n, n)
        dispatch_arrival(s).wait_recv()
        ans[s] = expert(recv[s])
        answer_copy(s).start()
        return c

    lax.fori_loop(0, n - 1, serve, 0)

    def mix(i, total):
        j = lax.rem(tp + i, nt)
        part_arrival(j).wait_recv()
        return total + prec[j].astype(F32)

    projected = pout[tp].astype(F32)
    for i in range(1, nt):
        projected = mix(i, projected)
    mixed_ref[...] = rms(projected, ps_ref[...]).astype(BF16)

    def weigh(e, block):
        lane = lane_c + e * cap
        w = jnp.where(lane == slot_a, rw_a, jnp.where(lane == slot_b, rw_b, 0.0))
        high = w.astype(BF16)
        low = (w - high.astype(F32)).astype(BF16)
        return dot(high, block) + dot(low, block)

    acc[...] = weigh(me, ans[me])

    def collect(i, c):
        e = lax.rem(me + offset(i), n)
        answer_arrival(e).wait_recv()
        acc[...] += weigh(e, back[e])
        return c

    lax.fori_loop(0, n - 1, collect, 0)
    routed_ref[...] = acc[...].astype(BF16)

    def finish(i, c):
        e = lax.rem(me + i, n)
        dispatch_copy(e).wait_send()
        answer_copy(e).wait_send()
        return c

    lax.fori_loop(1, n, finish, 0)

    def finish_group(g, c):
        for copy in group_copies(g):
            copy.wait_send()
        return c

    lax.fori_loop(grp + 1, groups, finish_group, 0)
    for i in range(1, nt):
        part_copy(lax.rem(tp + i, nt)).wait_send()


def relay_kernel(
    n, nt, cap,
    q_ref, k_ref, v_ref, ig_ref, fg_ref, fb_ref, hs_ref, wo_hbm, ps_ref,
    x_ref, es_ref, ids_ref, grp_ref, sc_ref, wg_hbm, wu_hbm, wd_hbm,
    mixed_ref, routed_ref,
    wg, wu, wd, wo, tok, info, xs, xr, ya, yb, own, part, ret, acc,
    cpair, spair, cgrp, sgrp, ent, head, pout, prec,
    wsem, t_ss, t_rs, i_ss, i_rs, x_ss, x_rs, y_ss, y_rs, r_ss, r_rs, c1s, c1r, s1s, s1r, c2s, c2r, s2s, s2r, p_ss, p_rs,
):
    me = lax.axis_index("ep")
    tp = lax.axis_index("tp")
    groups = n // 2
    grp = me // 2
    par = lax.rem(me, 2)
    partner = me + 1 - 2 * par
    tokens, width = x_ref.shape
    length, hd = q_ref.shape
    rows = mixed_ref.shape[0]

    barrier = pltpu.get_barrier_semaphore()

    def greet(i, c):
        pl.semaphore_signal(barrier, inc=1, device_id=(lax.rem(me + i, n), tp), device_id_type=MESH)
        return c

    lax.fori_loop(1, n, greet, 0)
    for j in range(1, nt):
        pl.semaphore_signal(barrier, inc=1, device_id=(me, lax.rem(tp + j, nt)), device_id_type=MESH)

    loads = [
        pltpu.make_async_copy(wg_hbm.at[0], wg, wsem.at[0]),
        pltpu.make_async_copy(wu_hbm.at[0], wu, wsem.at[1]),
        pltpu.make_async_copy(wd_hbm.at[0], wd, wsem.at[2]),
        pltpu.make_async_copy(wo_hbm.at[pl.ds(pl.multiple_of(tp * hd, hd), hd)], wo, wsem.at[3]),
    ]
    for load in loads:
        load.start()

    tok[grp] = rms(x_ref[...].astype(F32), es_ref[...]).astype(BF16)
    half = tokens // 2

    def tok_copy(s, h, to, sem):
        rows_of = pl.ds(h * half, half)
        return pltpu.make_async_remote_copy(
            src_ref=tok.at[s, rows_of], dst_ref=tok.at[s, rows_of], send_sem=t_ss.at[sem, h],
            recv_sem=t_rs.at[s, h], device_id=(to * 2 + par, tp), device_id_type=MESH)

    def info_copy(g, s):
        return pltpu.make_async_remote_copy(
            src_ref=info.at[s], dst_ref=info.at[s], send_sem=i_ss.at[g],
            recv_sem=i_rs.at[s], device_id=(g * 2 + par, tp), device_id_type=MESH)

    def swap_copy(kind, s):
        src, dst, ss, rs = ((xs, xr, x_ss, x_rs), (ya, yb, y_ss, y_rs))[kind]
        return pltpu.make_async_remote_copy(
            src_ref=src.at[s], dst_ref=dst.at[s], send_sem=ss.at[s],
            recv_sem=rs.at[s], device_id=(partner, tp), device_id_type=MESH)

    def ret_copy(s, slot, to):
        return pltpu.make_async_remote_copy(
            src_ref=part.at[s], dst_ref=ret.at[slot], send_sem=r_ss.at[s],
            recv_sem=r_rs.at[slot], device_id=(to * 2 + par, tp), device_id_type=MESH)


    pl.semaphore_wait(barrier, n - 1 + nt - 1)
    for h in range(2):
        @pl.when(grp + 1 < groups)
        def _():
            tok_copy(grp, h, grp + 1, grp).start()

        @pl.when(grp > 0)
        def _():
            tok_copy(grp, h, grp - 1, groups).start()

    ids = ids_ref[...]
    first, second = ids[:, 0:1], ids[:, 1:2]
    lane_e = lax.broadcasted_iota(jnp.int32, (tokens, n), 1)
    named = ((lane_e == first) | (lane_e == second)).astype(F32)
    tr = lax.broadcasted_iota(jnp.int32, (tokens, tokens), 0)
    tc = lax.broadcasted_iota(jnp.int32, (tokens, tokens), 1)
    rank = dot((tc < tr).astype(BF16), named.astype(BF16))
    slot_a = first * cap + jnp.sum(jnp.where(lane_e == first, rank, 0.0), axis=1, keepdims=True).astype(jnp.int32)
    slot_b = second * cap + jnp.sum(jnp.where(lane_e == second, rank, 0.0), axis=1, keepdims=True).astype(jnp.int32)
    score = sc_ref[...]
    ex = jnp.exp(score - jnp.max(score, axis=-1, keepdims=True))
    route = grp_ref[...] * (ex / jnp.sum(ex, axis=-1, keepdims=True))
    rw_a, rw_b = route[:, 0:1], route[:, 1:2]
    lane_c = lax.broadcasted_iota(jnp.int32, (tokens, cap), 1)

    lane_i = lax.broadcasted_iota(jnp.int32, (tokens, 128), 1)
    table = jnp.where(lane_i == 0, slot_a.astype(F32), jnp.where(lane_i == 1, slot_b.astype(F32),
        jnp.where(lane_i == 2, rw_a, jnp.where(lane_i == 3, rw_b, 0.0))))
    wide = info.shape[2]
    table = jnp.concatenate([table, jnp.zeros((wide - tokens, 128), F32)], axis=0)
    info[grp] = table.T[0:8]

    def send_info(j, c):
        info_copy(lax.rem(grp + j, groups), grp).start()
        return c

    lax.fori_loop(1, groups, send_info, 0)

    def columns(s):
        wide_cols = jnp.concatenate([info[s], jnp.zeros((120, info.shape[2]), F32)], axis=0).T[0:tokens]
        return (wide_cols[:, 0:1].astype(jnp.int32), wide_cols[:, 1:2].astype(jnp.int32),
                wide_cols[:, 2:3], wide_cols[:, 3:4])

    def place(cols_s, e):
        lane = lane_c + e * cap
        return ((lane == cols_s[0]) | (lane == cols_s[1])).astype(BF16)

    def pack(s):
        xs[s] = dot(place(columns(s), partner), tok[s], ((0,), (0,))).astype(BF16)
        swap_copy(0, s).start()

    pack(grp)

    fg = fg_ref[...]
    lk = jnp.minimum(fg, 0.0) - jnp.log1p(jnp.exp(-jnp.abs(fg))) + fb_ref[...]
    rid = lax.broadcasted_iota(jnp.int32, (length, length), 0)
    cid = lax.broadcasted_iota(jnp.int32, (length, length), 1)
    upper = (rid <= cid).astype(F32)
    b_row = dot(jnp.broadcast_to(lk, (8, length)), upper, precision=lax.Precision.HIGHEST)[0:1]
    i_row = ig_ref[...]
    last = b_row[:, length - 1 : length]
    g_row = last - b_row + i_row
    m_loc = jnp.max(g_row, axis=-1, keepdims=True)
    which = lax.broadcasted_iota(jnp.int32, (128, length), 0)
    cols = jnp.where(which == 0, b_row, g_row).T
    b_col = cols[:, 0:1]
    g_col = cols[:, 1:2]
    kw = k_ref[...].astype(F32) * (jnp.exp(g_col - m_loc) * (hd**-0.5))
    c_loc = dot(kw.astype(BF16), v_ref[...], ((0,), (0,)))
    n_loc = jnp.sum(kw, axis=0, keepdims=True)
    stat_id = lax.broadcasted_iota(jnp.int32, (8, hd), 0)

    def stats(total, peak, nor):
        return jnp.where(stat_id == 0, nor, jnp.where(stat_id == 1, peak, total))

    cpair[par] = c_loc.astype(BF16)
    spair[par] = stats(last, m_loc, n_loc)

    def pair_copies():
        return [
            pltpu.make_async_remote_copy(
                src_ref=cpair.at[par], dst_ref=cpair.at[par], send_sem=c1s, recv_sem=c1r,
                device_id=(partner, tp), device_id_type=MESH),
            pltpu.make_async_remote_copy(
                src_ref=spair.at[par], dst_ref=spair.at[par], send_sem=s1s, recv_sem=s1r,
                device_id=(partner, tp), device_id_type=MESH),
        ]

    for copy in pair_copies():
        copy.start()

    for copy in pair_copies():
        copy.wait_send()
    def pair_arrival():
        return [
            pltpu.make_async_remote_copy(
                src_ref=cpair.at[1 - par], dst_ref=cpair.at[1 - par], send_sem=c1s, recv_sem=c1r,
                device_id=(partner, tp), device_id_type=MESH),
            pltpu.make_async_remote_copy(
                src_ref=spair.at[1 - par], dst_ref=spair.at[1 - par], send_sem=s1s, recv_sem=s1r,
                device_id=(partner, tp), device_id_type=MESH),
        ]

    for copy in pair_arrival():
        copy.wait_recv()

    def unpack(c, s):
        return (s[2:3], s[1:2], c.astype(F32), s[0:1])

    both = join(unpack(cpair[0], spair[0]), unpack(cpair[1], spair[1]))
    cgrp[grp] = both[2].astype(BF16)
    sgrp[grp] = stats(both[0], both[1], both[3])

    def group_copies(g):
        to = (g * 2 + par, tp)
        return [
            pltpu.make_async_remote_copy(
                src_ref=cgrp.at[grp], dst_ref=cgrp.at[grp], send_sem=c2s.at[g], recv_sem=c2r.at[grp],
                device_id=to, device_id_type=MESH),
            pltpu.make_async_remote_copy(
                src_ref=sgrp.at[grp], dst_ref=sgrp.at[grp], send_sem=s2s.at[g], recv_sem=s2r.at[grp],
                device_id=to, device_id_type=MESH),
        ]

    def group_arrivals(g):
        at = (g * 2 + par, tp)
        return [
            pltpu.make_async_remote_copy(
                src_ref=cgrp.at[g], dst_ref=cgrp.at[g], send_sem=c2s.at[g], recv_sem=c2r.at[g],
                device_id=at, device_id_type=MESH),
            pltpu.make_async_remote_copy(
                src_ref=sgrp.at[g], dst_ref=sgrp.at[g], send_sem=s2s.at[g], recv_sem=s2r.at[g],
                device_id=at, device_id_type=MESH),
        ]

    def send_group(g, c):
        for copy in group_copies(g):
            copy.start()
        return c

    lax.fori_loop(grp + 1, groups, send_group, 0)

    for load in loads:
        load.wait()

    def weigh(cols_s, e, block):
        lane = lane_c + e * cap
        w = jnp.where(lane == cols_s[0], cols_s[2], jnp.where(lane == cols_s[1], cols_s[3], 0.0))
        high = w.astype(BF16)
        low = (w - high.astype(F32)).astype(BF16)
        return dot(high, block) + dot(low, block)

    def experts(s):
        cols_s = columns(s)
        mine = dot(place(cols_s, me), tok[s], ((0,), (0,))).astype(BF16)
        swap_copy(0, s).wait_recv()
        chosen = jnp.concatenate([xr[s], mine], axis=0)
        gate = dot(chosen, wg[...])
        up = dot(chosen, wu[...])
        hidden = (gate / (1.0 + jnp.exp(-gate)) * up).astype(BF16)
        answer = dot(hidden, wd[...]).astype(BF16)
        ya[s] = answer[0:cap]
        swap_copy(1, s).start()
        own[s] = answer[cap:]

    def combined(s):
        cols_s = columns(s)
        swap_copy(1, s).wait_recv()
        return weigh(cols_s, me, own[s]) + weigh(cols_s, partner, yb[s])

    def hop(s):
        below = s < grp
        to = jnp.where(below, grp - 1, grp + 1)
        slot = jnp.where(to == s, jnp.where(below, s, groups), s)
        return ret_copy(s, slot, to)

    def where_is(i):
        d, side = 1 + i // 2, lax.rem(i, 2)
        s = grp + d * (2 * side - 1)
        return s, (s >= 0) & (s < groups)

    def at_end(s):
        return jnp.where(s < grp, grp == groups - 1, grp == 0)

    def take(i, c):
        s, valid = where_is(i)

        @pl.when(valid)
        def _():
            onward = jnp.where(s < grp, grp + 1, grp - 1)
            for h in range(2):
                tok_copy(s, h, grp, s).wait_recv()

                @pl.when(jnp.logical_not(at_end(s)))
                def _():
                    tok_copy(s, h, onward, s).start()

            info_copy(s, s).wait_recv()
            pack(s)

        return c

    def work(i, c):
        s, valid = where_is(i)

        @pl.when(valid)
        def _():
            experts(s)

        return c

    def close(i, c):
        s, valid = where_is(i)

        @pl.when(valid & at_end(s))
        def _():
            part[s] = combined(s).astype(BF16)
            hop(s).start()

        return c

    def serve(d, c):
        for step in (take, work, close):
            lax.fori_loop(2 * d, 2 * d + 2, step, 0)
        return c

    experts(grp)
    lax.fori_loop(0, 1, serve, 0)

    ent[...] = jnp.zeros(ent.shape, F32)
    row1 = jnp.zeros((1, hd), F32)

    def enter(g, carry):
        total, peak, nor = carry
        for copy in group_arrivals(g):
            copy.wait_recv()
        total, peak, mem, nor = join((total, peak, ent[...], nor), unpack(cgrp[g], sgrp[g]))
        ent[...] = mem
        return total, peak, nor

    total, peak, nor = lax.fori_loop(0, grp, enter, (row1, row1 + FLOOR, row1))
    joined = join((total, peak, ent[...], nor), unpack(cpair[0], spair[0]))
    odd = par == 1
    m_in = jnp.where(odd, joined[1], peak)
    n_in = jnp.where(odd, joined[3], nor)
    c_in = jnp.where(odd, joined[2], ent[...])

    carried = b_col + m_in[:, 0:1]
    decay = jnp.where(cid <= rid, b_col - b_row + i_row, -jnp.inf)
    peaks = jnp.maximum(carried, jnp.max(decay, axis=-1, keepdims=True))
    across = jnp.exp(carried - peaks)
    scores = dot(q_ref[...], k_ref[...], ((1,), (1,))) * (hd**-0.5) * jnp.exp(decay - peaks)
    qf = q_ref[...].astype(F32)
    den = jnp.sum(scores, axis=-1, keepdims=True) + across * jnp.sum(qf * n_in, axis=-1, keepdims=True)
    num = dot(scores.astype(BF16), v_ref[...]) + across * dot(q_ref[...], c_in.astype(BF16))
    cell = num / jnp.maximum(jnp.abs(den), jnp.exp(-peaks))
    head[...] = (cell * hs_ref[...]).astype(BF16)

    def part_copy(j):
        return pltpu.make_async_remote_copy(
            src_ref=pout.at[j], dst_ref=prec.at[tp], send_sem=p_ss.at[j], recv_sem=p_rs.at[tp],
            device_id=(me, j), device_id_type=MESH)

    def part_arrival(j):
        return pltpu.make_async_remote_copy(
            src_ref=pout.at[j], dst_ref=prec.at[j], send_sem=p_ss.at[j], recv_sem=p_rs.at[j],
            device_id=(me, j), device_id_type=MESH)

    def project(j):
        pout[j] = dot(head[pl.ds(pl.multiple_of(j * rows, rows), rows), :], wo[...]).astype(BF16)

    def send_part(i, c):
        j = lax.rem(tp + i, nt)
        project(j)
        part_copy(j).start()
        return c

    lax.fori_loop(1, nt, send_part, 0)
    project(tp)

    lax.fori_loop(1, groups - 1, serve, 0)

    def give_back(j, c):
        s, valid = where_is(2 * (groups - 1) - 1 - j)

        @pl.when(valid & jnp.logical_not(at_end(s)))
        def _():
            mine = combined(s)
            ret_copy(s, s, grp).wait_recv()
            part[s] = (mine + ret[s].astype(F32)).astype(BF16)
            hop(s).start()

        return c

    lax.fori_loop(0, 2 * (groups - 1), give_back, 0)

    def mix(i, total):
        j = lax.rem(tp + i, nt)
        part_arrival(j).wait_recv()
        return total + prec[j].astype(F32)

    projected = pout[tp].astype(F32)
    for i in range(1, nt):
        projected = mix(i, projected)
    mixed_ref[...] = rms(projected, ps_ref[...]).astype(BF16)

    acc[...] = combined(grp)
    for slot, there in ((grp, grp + 1 < groups), (groups, grp > 0)):
        @pl.when(there)
        def _():
            ret_copy(grp, slot, grp).wait_recv()
            acc[...] += ret[slot].astype(F32)

    routed_ref[...] = acc[...].astype(BF16)

    def finish(s, c):
        swap_copy(0, s).wait_send()
        swap_copy(1, s).wait_send()

        @pl.when(s != grp)
        def _():
            hop(s).wait_send()
            info_copy(s, grp).wait_send()

        for h in range(2):
            @pl.when((s != grp) & jnp.logical_not(at_end(s)))
            def _():
                tok_copy(s, h, grp, s).wait_send()

        return c

    lax.fori_loop(0, groups, finish, 0)
    for h in range(2):
        @pl.when(grp + 1 < groups)
        def _():
            tok_copy(grp, h, grp, grp).wait_send()

        @pl.when(grp > 0)
        def _():
            tok_copy(grp, h, grp, groups).wait_send()

    def finish_group(g, c):
        for copy in group_copies(g):
            copy.wait_send()
        return c

    lax.fori_loop(grp + 1, groups, finish_group, 0)
    for i in range(1, nt):
        part_copy(lax.rem(tp + i, nt)).wait_send()


def shards(
    n, nt,
    memory_query_matrix, memory_key_matrix, memory_value_matrix,
    input_gate_logits, forget_gate_logits, forget_log_boosts,
    head_norm_scale, memory_output_matrix, projection_norm_scale,
    second_batch_rows, expert_prenorm_scale, selected_expert_index,
    group_route_probability, expert_choice_scores,
    expert_gate_matrix, expert_up_matrix, expert_down_matrix,
):
    length, hd = memory_query_matrix.shape
    tokens, width = second_batch_rows.shape
    hidden = expert_gate_matrix.shape[2]
    cap = 2 * selected_expert_index.shape[1] * tokens // n
    cap = -(-cap // 16) * 16
    rows = length // nt
    vm = pl.BlockSpec(memory_space=pltpu.VMEM)
    hbm = pl.BlockSpec(memory_space=pl.ANY)
    dma = pltpu.SemaphoreType.DMA
    slots = pltpu.VMEM((n, cap, width), BF16)
    groups = n // 2
    relay = groups * tokens * width * 6 < 24 * 1024 * 1024
    wide = -(-tokens // 128) * 128
    some = pltpu.VMEM((groups, cap, width), BF16)
    if relay:
        body = relay_kernel
        buffers = [
            pltpu.VMEM((groups, tokens, width), BF16),
            pltpu.VMEM((groups, 8, wide), F32),
            some, some, some, some, some,
            pltpu.VMEM((groups, tokens, width), BF16),
            pltpu.VMEM((groups + 1, tokens, width), BF16),
            pltpu.VMEM((tokens, width), F32),
        ]
        sems = [dma((groups + 1, 2)), dma((groups, 2))] + [dma((groups,))] * 7 + [dma((groups + 1,))]
    else:
        body = kernel
        buffers = [
            slots, slots, slots, slots,
            pltpu.VMEM((tokens, width), BF16),
            pltpu.VMEM((tokens, width), F32),
        ]
        sems = [dma((n,))] * 4
    return pl.pallas_call(
        functools.partial(body, n, nt, cap),
        out_shape=(
            jax.ShapeDtypeStruct((rows, width), BF16),
            jax.ShapeDtypeStruct((tokens, width), BF16),
        ),
        in_specs=[vm] * 7 + [hbm] + [vm] * 6 + [hbm] * 3,
        out_specs=(vm, vm),
        scratch_shapes=[
            pltpu.VMEM((width, hidden), BF16),
            pltpu.VMEM((width, hidden), BF16),
            pltpu.VMEM((hidden, width), BF16),
            pltpu.VMEM((hd, width), BF16),
            *buffers,
            pltpu.VMEM((2, hd, hd), BF16),
            pltpu.VMEM((2, 8, hd), F32),
            pltpu.VMEM((n // 2, hd, hd), BF16),
            pltpu.VMEM((n // 2, 8, hd), F32),
            pltpu.VMEM((hd, hd), F32),
            pltpu.VMEM((length, hd), BF16),
            pltpu.VMEM((nt, rows, width), BF16),
            pltpu.VMEM((nt, rows, width), BF16),
            dma((4,)),
            *sems,
            dma, dma, dma, dma,
            dma((n // 2,)), dma((n // 2,)), dma((n // 2,)), dma((n // 2,)),
            dma((nt,)), dma((nt,)),
        ],
        compiler_params=pltpu.CompilerParams(
            collective_id=0, has_side_effects=True, vmem_limit_bytes=62 * 1024 * 1024
        ),
    )(
        memory_query_matrix, memory_key_matrix, memory_value_matrix,
        input_gate_logits, forget_gate_logits, forget_log_boosts,
        head_norm_scale[None], memory_output_matrix, projection_norm_scale[None],
        second_batch_rows, expert_prenorm_scale[None], selected_expert_index,
        group_route_probability[:, None], expert_choice_scores,
        expert_gate_matrix, expert_up_matrix, expert_down_matrix,
    )


def solution(mesh):
    return jax.shard_map(
        functools.partial(shards, mesh.shape["ep"], mesh.shape["tp"]),
        mesh=mesh,
        in_specs=(
            P("ep", "tp"), P("ep", "tp"), P("ep", "tp"),
            P("tp", "ep"), P("tp", "ep"), P("tp", "ep"),
            P("tp"), P(), P(),
            P(("ep", "tp"), None), P(), P(("ep", "tp"), None),
            P(("ep", "tp")), P(("ep", "tp"), None),
            P("ep", None, None), P("ep", None, None), P("ep", None, None),
        ),
        out_specs=(P(("ep", "tp"), None), P(("ep", "tp"), None)),
        check_vma=False,
    )
```

profile of v0, /device:TPU:0, one launch (start us, length us, event | category | flops | bytes accessed | tf_op | source)
XLA Modules:
  0.0 150.3 jit_solution(3609801528914307580)
XLA Ops:
  0.6 1.4 copy.21.ids_ref
  2.1 1.4 copy.22.grp_ref
  3.5 1.4 copy.23.sc_ref
  5.0 141.3 %shard_map.176 = (bf16[128,2048]{1,0:T(8,128)(2,1)}, bf16[192,2048]{1,0:T(8,128)(2,1)}) custom-call(bf16[512,256]{1,0:T(8,128)(2,1)} %q_ref.1, bf16[512,256]{1,0:T(8,128)(2,1)} %k_ref.1, bf16[512,256]{1,0:T(8,128)(2,1)} %v_ref.1, f32[1,512]{1,0:T(1,128)} %ig_ref.1, f32[1,512]{1,0:T(1,128)} %fg_ref.1, f32[1,512]{1,0:T(1,128)} %fb_ref.1, f32[1,256]{1,0:T(1,128)} %bitcast.7, ...), custom_call_target="tpu_custom_call" | custom-call | tf_op jit(solution)/shard_map/pallas_call | solution.py:790
  146.3 1.9 %copy.26 = bf16[128,2048]{1,0:T(8,128)(2,1)} copy(bf16[128,2048]{1,0:T(8,128)(2,1)} %get-tuple-element.4) | data formatting | bytes 1048576
  148.2 2.1 %copy.27 = bf16[192,2048]{1,0:T(8,128)(2,1)} copy(bf16[192,2048]{1,0:T(8,128)(2,1)} %get-tuple-element.5) | data formatting | bytes 1572864
where the time goes:
time: 151 us; the launch traced here: 150 us
  Pallas kernels  141 us (93%)
  local copies, waits for them, and re-layouts  8.3 us (5%)
    pallas_call x1, Pallas kernels, shards(): pl.pallas_call(functools.partial(body, n, nt, cap), out_shape=(jax.ShapeD...  141 us
    unnamed x4, local copies, waits for them, and re-layouts  6.86 us

commit v1 on v0

--- a/solution.py
+++ b/solution.py
@@ -330,24 +330,32 @@
         part_copy(lax.rem(tp + i, nt)).wait_send()
 
 
-def relay_kernel(
-    n, nt, cap,
+def plane_kernel(
+    n, nt, cap, nc,
     q_ref, k_ref, v_ref, ig_ref, fg_ref, fb_ref, hs_ref, wo_hbm, ps_ref,
     x_ref, es_ref, ids_ref, grp_ref, sc_ref, wg_hbm, wu_hbm, wd_hbm,
     mixed_ref, routed_ref,
-    wg, wu, wd, wo, tok, info, xs, xr, ya, yb, own, part, ret, acc,
-    cpair, spair, cgrp, sgrp, ent, head, pout, prec,
-    wsem, t_ss, t_rs, i_ss, i_rs, x_ss, x_rs, y_ss, y_rs, r_ss, r_rs, c1s, c1r, s1s, s1r, c2s, c2r, s2s, s2r, p_ss, p_rs,
+    wg, wu, wd, wo, tok, info, chosen, hid, ans, cin, rout, rin, acc,
+    cpair, spair, cgrp, sgrp, cpre, spre, ent, num, stat, head, pout, prec,
+    wsem, x_ss, y_ss, k_ss, w_rs, t_ss, t_rs, i_ss, i_rs, c_ss, c_rs, r_ss, r_rs,
+    c1s, c1r, s1s, s1r, c2s, c2r, s2s, s2r, p_ss, p_rs,
 ):
     me = lax.axis_index("ep")
     tp = lax.axis_index("tp")
     groups = n // 2
-    grp = me // 2
+    z = me // 2
     par = lax.rem(me, 2)
     partner = me + 1 - 2 * par
+    other = tp + 1 - 2 * lax.rem(tp, 2)
     tokens, width = x_ref.shape
     length, hd = q_ref.shape
     rows = mixed_ref.shape[0]
+    cw = width // nc
+    pieces = 3 * nc
+
+    def remote(src, dst, ss, rs, to):
+        return pltpu.make_async_remote_copy(
+            src_ref=src, dst_ref=dst, send_sem=ss, recv_sem=rs, device_id=to, device_id_type=MESH)
 
     barrier = pltpu.get_barrier_semaphore()
 
@@ -360,92 +368,124 @@
         pl.semaphore_signal(barrier, inc=1, device_id=(me, lax.rem(tp + j, nt)), device_id_type=MESH)
 
     loads = [
-        pltpu.make_async_copy(wg_hbm.at[0], wg, wsem.at[0]),
-        pltpu.make_async_copy(wu_hbm.at[0], wu, wsem.at[1]),
-        pltpu.make_async_copy(wd_hbm.at[0], wd, wsem.at[2]),
+        pltpu.make_async_copy(wg_hbm.at[0], wg.at[0], wsem.at[0]),
+        pltpu.make_async_copy(wu_hbm.at[0], wu.at[0], wsem.at[1]),
+        pltpu.make_async_copy(wd_hbm.at[0], wd.at[0], wsem.at[2]),
         pltpu.make_async_copy(wo_hbm.at[pl.ds(pl.multiple_of(tp * hd, hd), hd)], wo, wsem.at[3]),
     ]
     for load in loads:
         load.start()
 
-    tok[grp] = rms(x_ref[...].astype(F32), es_ref[...]).astype(BF16)
-    half = tokens // 2
-
-    def tok_copy(s, h, to, sem):
-        rows_of = pl.ds(h * half, half)
-        return pltpu.make_async_remote_copy(
-            src_ref=tok.at[s, rows_of], dst_ref=tok.at[s, rows_of], send_sem=t_ss.at[sem, h],
-            recv_sem=t_rs.at[s, h], device_id=(to * 2 + par, tp), device_id_type=MESH)
-
-    def info_copy(g, s):
-        return pltpu.make_async_remote_copy(
-            src_ref=info.at[s], dst_ref=info.at[s], send_sem=i_ss.at[g],
-            recv_sem=i_rs.at[s], device_id=(g * 2 + par, tp), device_id_type=MESH)
-
-    def swap_copy(kind, s):
-        src, dst, ss, rs = ((xs, xr, x_ss, x_rs), (ya, yb, y_ss, y_rs))[kind]
-        return pltpu.make_async_remote_copy(
-            src_ref=src.at[s], dst_ref=dst.at[s], send_sem=ss.at[s],
-            recv_sem=rs.at[s], device_id=(partner, tp), device_id_type=MESH)
-
-    def ret_copy(s, slot, to):
-        return pltpu.make_async_remote_copy(
-            src_ref=part.at[s], dst_ref=ret.at[slot], send_sem=r_ss.at[s],
-            recv_sem=r_rs.at[slot], device_id=(to * 2 + par, tp), device_id_type=MESH)
-
+    def piece(ref, lead, part, j):
+        which, at = divmod(j, nc)
+        if which < 2:
+            quarter = ref[which].shape[1] // nt
+            step = quarter // nc
+            return ref[which].at[lead, pl.ds(pl.multiple_of(part * quarter + at * step, step), step)]
+        quarter = ref[2].shape[1] // nt
+        step = width // nc
+        return ref[2].at[lead, pl.ds(pl.multiple_of(part * quarter, quarter), quarter), pl.ds(at * step, step)]
+
+    held = (wg, wu, wd)
+    given = (wg_hbm, wu_hbm, wd_hbm)
+
+    def x_copy(j):
+        return remote(piece(given, 0, tp, j), piece(held, 1, tp, j), x_ss.at[j], w_rs.at[tp, j], (partner, tp))
+
+    def y_copy(o, j):
+        here = piece(held, 1, tp, j)
+        return remote(here, here, y_ss.at[o, j], w_rs.at[tp, j], (me, lax.rem(tp + 2 * o, nt)))
+
+    def core_copy(part, j):
+        here = piece(held, 1, part, j)
+        return remote(here, here, k_ss.at[part // 2, j], w_rs.at[part, j], (me, other))
+
+    def weight_wait(part, j):
+        here = piece(held, 1, part, j)
+        remote(here, here, x_ss.at[j], w_rs.at[part, j], (me, other)).wait_recv()
+
+    def from_partner(j):
+        weight_wait(tp, j)
+        for o in range(1, nt // 2):
+            y_copy(o, j).start()
+        core_copy(tp, j).start()
+
+    def from_peers(j):
+        for o in range(1, nt // 2):
+            part = lax.rem(tp + 2 * o, nt)
+            weight_wait(part, j)
+            core_copy(part, j).start()
+
+    def from_core(j):
+        for o in range(nt // 2):
+            weight_wait(lax.rem(other + 2 * o, nt), j)
+
+    def tok_copy(up, s, c):
+        here = tok.at[s, c]
+        return remote(here, here, t_ss.at[up, s, c], t_rs.at[s, c], ((z - 1 + 2 * up) * 2 + par, tp))
+
+    def tok_wait(s, c):
+        here = tok.at[s, c]
+        remote(here, here, t_ss.at[0, s, c], t_rs.at[s, c], (me, other)).wait_recv()
+
+    def send_own(c):
+        @pl.when(z + 1 < groups)
+        def _():
+            tok_copy(1, z, c).start()
+
+        @pl.when(z > 0)
+        def _():
+            tok_copy(0, z, c).start()
+
+    def forward(i, c):
+        @pl.when((z - 1 - i >= 0) & (z + 1 < groups))
+        def _():
+            tok_wait(z - 1 - i, c)
+            tok_copy(1, z - 1 - i, c).start()
+
+        @pl.when((z + 1 + i < groups) & (z > 0))
+        def _():
+            tok_wait(z + 1 + i, c)
+            tok_copy(0, z + 1 + i, c).start()
+
+    normed = rms(x_ref[...].astype(F32), es_ref[...]).astype(BF16)
+    for c in range(nc):
+        tok[z, c] = normed[:, c * cw : (c + 1) * cw]
 
     pl.semaphore_wait(barrier, n - 1 + nt - 1)
-    for h in range(2):
-        @pl.when(grp + 1 < groups)
-        def _():
-            tok_copy(grp, h, grp + 1, grp).start()
-
-        @pl.when(grp > 0)
-        def _():
-            tok_copy(grp, h, grp - 1, groups).start()
-
-    ids = ids_ref[...]
-    first, second = ids[:, 0:1], ids[:, 1:2]
-    lane_e = lax.broadcasted_iota(jnp.int32, (tokens, n), 1)
-    named = ((lane_e == first) | (lane_e == second)).astype(F32)
+    early = nc // 2
+    for c in range(early):
+        send_own(c)
+    for j in range(2):
+        x_copy(j).start()
+
+    first, second = ids_ref[0:1, :], ids_ref[1:2, :]
+    sub_e = lax.broadcasted_iota(jnp.int32, (n, tokens), 0)
+    named = ((sub_e == first) | (sub_e == second)).astype(BF16)
     tr = lax.broadcasted_iota(jnp.int32, (tokens, tokens), 0)
     tc = lax.broadcasted_iota(jnp.int32, (tokens, tokens), 1)
-    rank = dot((tc < tr).astype(BF16), named.astype(BF16))
-    slot_a = first * cap + jnp.sum(jnp.where(lane_e == first, rank, 0.0), axis=1, keepdims=True).astype(jnp.int32)
-    slot_b = second * cap + jnp.sum(jnp.where(lane_e == second, rank, 0.0), axis=1, keepdims=True).astype(jnp.int32)
-    score = sc_ref[...]
-    ex = jnp.exp(score - jnp.max(score, axis=-1, keepdims=True))
-    route = grp_ref[...] * (ex / jnp.sum(ex, axis=-1, keepdims=True))
-    rw_a, rw_b = route[:, 0:1], route[:, 1:2]
-    lane_c = lax.broadcasted_iota(jnp.int32, (tokens, cap), 1)
-
-    lane_i = lax.broadcasted_iota(jnp.int32, (tokens, 128), 1)
-    table = jnp.where(lane_i == 0, slot_a.astype(F32), jnp.where(lane_i == 1, slot_b.astype(F32),
-        jnp.where(lane_i == 2, rw_a, jnp.where(lane_i == 3, rw_b, 0.0))))
-    wide = info.shape[2]
-    table = jnp.concatenate([table, jnp.zeros((wide - tokens, 128), F32)], axis=0)
-    info[grp] = table.T[0:8]
+    rank = dot(named, (tr < tc).astype(BF16))
+    slot_a = first.astype(F32) * cap + jnp.sum(jnp.where(sub_e == first, rank, 0.0), axis=0, keepdims=True)
+    slot_b = second.astype(F32) * cap + jnp.sum(jnp.where(sub_e == second, rank, 0.0), axis=0, keepdims=True)
+    score_a, score_b = sc_ref[0:1, :], sc_ref[1:2, :]
+    top = jnp.maximum(score_a, score_b)
+    ex_a, ex_b = jnp.exp(score_a - top), jnp.exp(score_b - top)
+    rw_a = grp_ref[...] * (ex_a / (ex_a + ex_b))
+    rw_b = grp_ref[...] * (ex_b / (ex_a + ex_b))
+    sub_i = lax.broadcasted_iota(jnp.int32, (8, tokens), 0)
+    table = jnp.where(sub_i == 0, slot_a, jnp.where(sub_i == 1, slot_b,
+        jnp.where(sub_i == 2, rw_a, jnp.where(sub_i == 3, rw_b, 0.0))))
+    info[z] = jnp.zeros(info.shape[1:], F32)
+    info[z, :, 0:tokens] = table
+
+    def info_copy(g, s):
+        return remote(info.at[s], info.at[s], i_ss.at[g], i_rs.at[s], (g * 2 + par, tp))
 
     def send_info(j, c):
-        info_copy(lax.rem(grp + j, groups), grp).start()
+        info_copy(lax.rem(z + j, groups), z).start()
         return c
 
     lax.fori_loop(1, groups, send_info, 0)
-
-    def columns(s):
-        wide_cols = jnp.concatenate([info[s], jnp.zeros((120, info.shape[2]), F32)], axis=0).T[0:tokens]
-        return (wide_cols[:, 0:1].astype(jnp.int32), wide_cols[:, 1:2].astype(jnp.int32),
-                wide_cols[:, 2:3], wide_cols[:, 3:4])
-
-    def place(cols_s, e):
-        lane = lane_c + e * cap
-        return ((lane == cols_s[0]) | (lane == cols_s[1])).astype(BF16)
-
-    def pack(s):
-        xs[s] = dot(place(columns(s), partner), tok[s], ((0,), (0,))).astype(BF16)
-        swap_copy(0, s).start()
-
-    pack(grp)
 
     fg = fg_ref[...]
     lk = jnp.minimum(fg, 0.0) - jnp.log1p(jnp.exp(-jnp.abs(fg))) + fb_ref[...]
@@ -457,210 +497,107 @@
     last = b_row[:, length - 1 : length]
     g_row = last - b_row + i_row
     m_loc = jnp.max(g_row, axis=-1, keepdims=True)
-    which = lax.broadcasted_iota(jnp.int32, (128, length), 0)
-    cols = jnp.where(which == 0, b_row, g_row).T
-    b_col = cols[:, 0:1]
-    g_col = cols[:, 1:2]
-    kw = k_ref[...].astype(F32) * (jnp.exp(g_col - m_loc) * (hd**-0.5))
-    c_loc = dot(kw.astype(BF16), v_ref[...], ((0,), (0,)))
+    which_row = lax.broadcasted_iota(jnp.int32, (128, length), 0)
+    stat[...] = jnp.where(which_row == 0, b_row, g_row).T
+    kw = k_ref[...].astype(F32) * (jnp.exp(stat[:, 1:2] - m_loc) * (hd**-0.5))
     n_loc = jnp.sum(kw, axis=0, keepdims=True)
     stat_id = lax.broadcasted_iota(jnp.int32, (8, hd), 0)
 
     def stats(total, peak, nor):
         return jnp.where(stat_id == 0, nor, jnp.where(stat_id == 1, peak, total))
 
-    cpair[par] = c_loc.astype(BF16)
-    spair[par] = stats(last, m_loc, n_loc)
-
-    def pair_copies():
-        return [
-            pltpu.make_async_remote_copy(
-                src_ref=cpair.at[par], dst_ref=cpair.at[par], send_sem=c1s, recv_sem=c1r,
-                device_id=(partner, tp), device_id_type=MESH),
-            pltpu.make_async_remote_copy(
-                src_ref=spair.at[par], dst_ref=spair.at[par], send_sem=s1s, recv_sem=s1r,
-                device_id=(partner, tp), device_id_type=MESH),
-        ]
-
-    for copy in pair_copies():
-        copy.start()
-
-    for copy in pair_copies():
-        copy.wait_send()
-    def pair_arrival():
-        return [
-            pltpu.make_async_remote_copy(
-                src_ref=cpair.at[1 - par], dst_ref=cpair.at[1 - par], send_sem=c1s, recv_sem=c1r,
-                device_id=(partner, tp), device_id_type=MESH),
-            pltpu.make_async_remote_copy(
-                src_ref=spair.at[1 - par], dst_ref=spair.at[1 - par], send_sem=s1s, recv_sem=s1r,
-                device_id=(partner, tp), device_id_type=MESH),
-        ]
-
-    for copy in pair_arrival():
-        copy.wait_recv()
-
     def unpack(c, s):
         return (s[2:3], s[1:2], c.astype(F32), s[0:1])
 
-    both = join(unpack(cpair[0], spair[0]), unpack(cpair[1], spair[1]))
-    cgrp[grp] = both[2].astype(BF16)
-    sgrp[grp] = stats(both[0], both[1], both[3])
-
-    def group_copies(g):
-        to = (g * 2 + par, tp)
+    cpair[par] = dot(kw.astype(BF16), v_ref[...], ((0,), (0,))).astype(BF16)
+    spair[par] = stats(last, m_loc, n_loc)
+
+    def pair_copies(at):
         return [
-            pltpu.make_async_remote_copy(
-                src_ref=cgrp.at[grp], dst_ref=cgrp.at[grp], send_sem=c2s.at[g], recv_sem=c2r.at[grp],
-                device_id=to, device_id_type=MESH),
-            pltpu.make_async_remote_copy(
-                src_ref=sgrp.at[grp], dst_ref=sgrp.at[grp], send_sem=s2s.at[g], recv_sem=s2r.at[grp],
-                device_id=to, device_id_type=MESH),
+            remote(cpair.at[at], cpair.at[at], c1s, c1r, (partner, tp)),
+            remote(spair.at[at], spair.at[at], s1s, s1r, (partner, tp)),
         ]
 
-    def group_arrivals(g):
-        at = (g * 2 + par, tp)
+    for copy in pair_copies(par):
+        copy.start()
+    for j in range(2, pieces):
+        x_copy(j).start()
+    for c in range(early, nc):
+        send_own(c)
+
+    def pre_copies():
+        to = ((z + 1) * 2 + par, tp)
         return [
-            pltpu.make_async_remote_copy(
-                src_ref=cgrp.at[g], dst_ref=cgrp.at[g], send_sem=c2s.at[g], recv_sem=c2r.at[g],
-                device_id=at, device_id_type=MESH),
-            pltpu.make_async_remote_copy(
-                src_ref=sgrp.at[g], dst_ref=sgrp.at[g], send_sem=s2s.at[g], recv_sem=s2r.at[g],
-                device_id=at, device_id_type=MESH),
+            remote(cpre.at[1], cpre.at[0], c2s, c2r, to),
+            remote(spre.at[1], spre.at[0], s2s, s2r, to),
         ]
 
-    def send_group(g, c):
-        for copy in group_copies(g):
-            copy.start()
-        return c
-
-    lax.fori_loop(grp + 1, groups, send_group, 0)
-
-    for load in loads:
-        load.wait()
-
-    def weigh(cols_s, e, block):
-        lane = lane_c + e * cap
-        w = jnp.where(lane == cols_s[0], cols_s[2], jnp.where(lane == cols_s[1], cols_s[3], 0.0))
-        high = w.astype(BF16)
-        low = (w - high.astype(F32)).astype(BF16)
-        return dot(high, block) + dot(low, block)
-
-    def experts(s):
-        cols_s = columns(s)
-        mine = dot(place(cols_s, me), tok[s], ((0,), (0,))).astype(BF16)
-        swap_copy(0, s).wait_recv()
-        chosen = jnp.concatenate([xr[s], mine], axis=0)
-        gate = dot(chosen, wg[...])
-        up = dot(chosen, wu[...])
-        hidden = (gate / (1.0 + jnp.exp(-gate)) * up).astype(BF16)
-        answer = dot(hidden, wd[...]).astype(BF16)
-        ya[s] = answer[0:cap]
-        swap_copy(1, s).start()
-        own[s] = answer[cap:]
-
-    def combined(s):
-        cols_s = columns(s)
-        swap_copy(1, s).wait_recv()
-        return weigh(cols_s, me, own[s]) + weigh(cols_s, partner, yb[s])
-
-    def hop(s):
-        below = s < grp
-        to = jnp.where(below, grp - 1, grp + 1)
-        slot = jnp.where(to == s, jnp.where(below, s, groups), s)
-        return ret_copy(s, slot, to)
-
-    def where_is(i):
-        d, side = 1 + i // 2, lax.rem(i, 2)
-        s = grp + d * (2 * side - 1)
-        return s, (s >= 0) & (s < groups)
-
-    def at_end(s):
-        return jnp.where(s < grp, grp == groups - 1, grp == 0)
-
-    def take(i, c):
-        s, valid = where_is(i)
-
-        @pl.when(valid)
-        def _():
-            onward = jnp.where(s < grp, grp + 1, grp - 1)
-            for h in range(2):
-                tok_copy(s, h, grp, s).wait_recv()
-
-                @pl.when(jnp.logical_not(at_end(s)))
-                def _():
-                    tok_copy(s, h, onward, s).start()
-
-            info_copy(s, s).wait_recv()
-            pack(s)
-
-        return c
-
-    def work(i, c):
-        s, valid = where_is(i)
-
-        @pl.when(valid)
-        def _():
-            experts(s)
-
-        return c
-
-    def close(i, c):
-        s, valid = where_is(i)
-
-        @pl.when(valid & at_end(s))
-        def _():
-            part[s] = combined(s).astype(BF16)
-            hop(s).start()
-
-        return c
-
-    def serve(d, c):
-        for step in (take, work, close):
-            lax.fori_loop(2 * d, 2 * d + 2, step, 0)
-        return c
-
-    experts(grp)
-    lax.fori_loop(0, 1, serve, 0)
-
-    ent[...] = jnp.zeros(ent.shape, F32)
-    row1 = jnp.zeros((1, hd), F32)
-
-    def enter(g, carry):
-        total, peak, nor = carry
-        for copy in group_arrivals(g):
+    def join_pair():
+        for copy in pair_copies(1 - par):
             copy.wait_recv()
-        total, peak, mem, nor = join((total, peak, ent[...], nor), unpack(cgrp[g], sgrp[g]))
-        ent[...] = mem
-        return total, peak, nor
-
-    total, peak, nor = lax.fori_loop(0, grp, enter, (row1, row1 + FLOOR, row1))
-    joined = join((total, peak, ent[...], nor), unpack(cpair[0], spair[0]))
-    odd = par == 1
-    m_in = jnp.where(odd, joined[1], peak)
-    n_in = jnp.where(odd, joined[3], nor)
-    c_in = jnp.where(odd, joined[2], ent[...])
-
-    carried = b_col + m_in[:, 0:1]
-    decay = jnp.where(cid <= rid, b_col - b_row + i_row, -jnp.inf)
-    peaks = jnp.maximum(carried, jnp.max(decay, axis=-1, keepdims=True))
-    across = jnp.exp(carried - peaks)
-    scores = dot(q_ref[...], k_ref[...], ((1,), (1,))) * (hd**-0.5) * jnp.exp(decay - peaks)
-    qf = q_ref[...].astype(F32)
-    den = jnp.sum(scores, axis=-1, keepdims=True) + across * jnp.sum(qf * n_in, axis=-1, keepdims=True)
-    num = dot(scores.astype(BF16), v_ref[...]) + across * dot(q_ref[...], c_in.astype(BF16))
-    cell = num / jnp.maximum(jnp.abs(den), jnp.exp(-peaks))
-    head[...] = (cell * hs_ref[...]).astype(BF16)
+        both = join(unpack(cpair[0], spair[0]), unpack(cpair[1], spair[1]))
+        cgrp[...] = both[2]
+        sgrp[...] = stats(both[0], both[1], both[3])
+
+    def hop(i):
+        @pl.when(z == i)
+        def _():
+            if i:
+                for copy in pre_copies():
+                    copy.wait_recv()
+                before = unpack(cpre[0], spre[0])
+                ent[...] = before[2]
+                sgate = spre[0]
+            else:
+                ent[...] = jnp.zeros(ent.shape, F32)
+                row1 = jnp.zeros((1, hd), F32)
+                sgate = stats(row1, row1 + FLOOR, row1)
+                spre[0] = sgate
+            if i + 1 < groups:
+                out = join((sgate[2:3], sgate[1:2], ent[...], sgate[0:1]), unpack(cgrp[...], sgrp[...]))
+                cpre[1] = out[2].astype(BF16)
+                spre[1] = stats(out[0], out[1], out[3])
+                for copy in pre_copies():
+                    copy.start()
+
+    rid_b = lax.broadcasted_iota(jnp.int32, (rows, length), 0)
+    cid_b = lax.broadcasted_iota(jnp.int32, (rows, length), 1)
+
+    def attend(r):
+        at, end = r * rows, (r + 1) * rows
+        decay = jnp.where(
+            cid_b[:, :end] <= rid_b[:, :end] + at, stat[at:end, 0:1] - b_row[:, :end] + i_row[:, :end], -jnp.inf)
+        peak = jnp.max(decay, axis=-1, keepdims=True)
+        scores = dot(q_ref[at:end], k_ref[0:end], ((1,), (1,))) * (hd**-0.5) * jnp.exp(decay - peak)
+        stat[at:end, 2:3] = peak
+        stat[at:end, 3:4] = jnp.sum(scores, axis=-1, keepdims=True)
+        num[at:end] = dot(scores.astype(BF16), v_ref[0:end])
+
+    def attend_end():
+        pre = (spre[0, 2:3], spre[0, 1:2], ent[...], spre[0, 0:1])
+        joined = join(pre, unpack(cpair[0], spair[0]))
+        odd = par == 1
+        m_in = jnp.where(odd, joined[1], pre[1])
+        n_in = jnp.where(odd, joined[3], pre[3])
+        c_in = jnp.where(odd, joined[2], pre[2]).astype(BF16)
+        for r in range(nt):
+            at, end = r * rows, (r + 1) * rows
+            carried = stat[at:end, 0:1] + m_in[:, 0:1]
+            local = stat[at:end, 2:3]
+            peaks = jnp.maximum(carried, local)
+            across = jnp.exp(carried - peaks)
+            within = jnp.exp(local - peaks)
+            qf = q_ref[at:end].astype(F32)
+            den = within * stat[at:end, 3:4] + across * jnp.sum(qf * n_in, axis=-1, keepdims=True)
+            top = within * num[at:end] + across * dot(q_ref[at:end], c_in)
+            cell = top / jnp.maximum(jnp.abs(den), jnp.exp(-peaks))
+            head[at:end] = (cell * hs_ref[...]).astype(BF16)
 
     def part_copy(j):
-        return pltpu.make_async_remote_copy(
-            src_ref=pout.at[j], dst_ref=prec.at[tp], send_sem=p_ss.at[j], recv_sem=p_rs.at[tp],
-            device_id=(me, j), device_id_type=MESH)
+        return remote(pout.at[j], prec.at[tp], p_ss.at[j], p_rs.at[tp], (me, j))
 
     def part_arrival(j):
-        return pltpu.make_async_remote_copy(
-            src_ref=pout.at[j], dst_ref=prec.at[j], send_sem=p_ss.at[j], recv_sem=p_rs.at[j],
-            device_id=(me, j), device_id_type=MESH)
+        return remote(pout.at[j], prec.at[j], p_ss.at[j], p_rs.at[j], (me, j))
 
     def project(j):
         pout[j] = dot(head[pl.ds(pl.multiple_of(j * rows, rows), rows), :], wo[...]).astype(BF16)
@@ -671,76 +608,310 @@
         part_copy(j).start()
         return c
 
+    def mix():
+        total = pout[tp].astype(F32)
+        for i in range(1, nt):
+            j = lax.rem(tp + i, nt)
+            part_arrival(j).wait_recv()
+            total = total + prec[j].astype(F32)
+        mixed_ref[...] = rms(total, ps_ref[...]).astype(BF16)
+
+    def masks(s, plane, start, count):
+        table = info[s]
+        slot = lax.broadcasted_iota(jnp.int32, (count, tokens), 0) + start
+        own = (plane * 2 + par) * cap
+        beside = (plane * 2 + 1 - par) * cap
+        slot = jnp.where(slot < cap, own + slot, beside + slot - cap).astype(F32)
+        return slot == table[0:1, 0:tokens], slot == table[1:2, 0:tokens], table[2:3, 0:tokens], table[3:4, 0:tokens]
+
+    def hidden(s, e, at):
+        is_a, is_b, _, _ = masks(s, z, e * cap, cap)
+        place = (is_a | is_b).astype(BF16)
+        for c in range(nc):
+            chosen[:, c * cw : (c + 1) * cw] = dot(place, tok[s, c]).astype(BF16)
+        gate = dot(chosen[...], wg[e])
+        up = dot(chosen[...], wu[e])
+        hid[at] = (gate / (1.0 + jnp.exp(-gate)) * up).astype(BF16)
+
+    def share(s, e):
+        is_a, is_b, w_a, w_b = masks(s, z, e * cap, cap)
+        return jnp.sum(jnp.where(is_a, w_a, jnp.where(is_b, w_b, 0.0)), axis=1, keepdims=True)
+
+    def half_of(e):
+        return pl.ds(pl.multiple_of(e * cap, 16), cap)
+
+    def down(s, e, at, c, weight):
+        answer = dot(hid[at], wd[e, :, c * cw : (c + 1) * cw]) * weight
+        ans[s, c, half_of(e), :] = answer.astype(BF16)
+
+    def ret_to(s):
+        below = s < z
+        to = jnp.where(below, z - 1, z + 1)
+        slot = jnp.where((to == s) & jnp.logical_not(below), groups, s)
+        return below, to, slot
+
+    def compact_copy(s, e, c):
+        _, to, slot = ret_to(s)
+        half = half_of(e)
+        return remote(ans.at[s, c, half], cin.at[slot, c, half], c_ss.at[s, e, c], c_rs.at[slot, e, c], (to * 2 + par, tp))
+
+    def compact_wait(slot, c):
+        for e in range(2):
+            half = half_of(e)
+            remote(ans.at[0, c, half], cin.at[slot, c, half], c_ss.at[0, e, c], c_rs.at[slot, e, c], (me, other)).wait_recv()
+
+    def sum_copy(s, c):
+        _, to, slot = ret_to(s)
+        return remote(rout.at[s, c], rin.at[slot, c], r_ss.at[s, c], r_rs.at[slot, c], (to * 2 + par, tp))
+
+    def sum_wait(slot, c):
+        remote(rout.at[0, c], rin.at[slot, c], r_ss.at[0, c], r_rs.at[slot, c], (me, other)).wait_recv()
+
+    def at_end(s):
+        return jnp.where(s < z, z == groups - 1, z == 0)
+
+    def valid(s):
+        return (s >= 0) & (s < groups)
+
+    def arrive(s):
+        @pl.when(at_end(s))
+        def _():
+            for c in range(nc):
+                tok_wait(s, c)
+
+        remote(info.at[s], info.at[s], i_ss.at[0], i_rs.at[s], (me, other)).wait_recv()
+
+    def answer(s, e, at):
+        hidden(s, e, at)
+        weight = share(s, e)
+        for c in range(nc):
+            down(s, e, at, c, weight)
+
+            @pl.when((s != z) & at_end(s))
+            def _():
+                compact_copy(s, e, c).start()
+
+    def scatter(s, plane, block):
+        is_a, is_b, _, _ = masks(s, plane, 0, 2 * cap)
+        return dot((is_a | is_b).astype(BF16), block, ((0,), (0,)))
+
+    def upstream(s, slot, near, last, c, put):
+        @pl.when(near == last)
+        def _():
+            compact_wait(slot, c)
+            put(scatter(s, last, cin[slot, c]))
+
+        @pl.when(near != last)
+        def _():
+            sum_wait(slot, c)
+            put(rin[slot, c].astype(F32))
+
+    def pass_on(s, c):
+        mine = scatter(s, z, ans[s, c])
+
+        def put(more):
+            rout[s, c] = (mine + more).astype(BF16)
+
+        below = s < z
+        upstream(s, s, jnp.where(below, z + 1, z - 1), jnp.where(below, groups - 1, 0), c, put)
+        sum_copy(s, c).start()
+
+    def own_end(c):
+        acc[...] = scatter(z, z, ans[z, c])
+
+        def put(more):
+            acc[...] += more
+
+        @pl.when(z < groups - 1)
+        def _():
+            upstream(z, z, z + 1, groups - 1, c, put)
+
+        @pl.when(z > 0)
+        def _():
+            upstream(z, groups, z - 1, 0, c, put)
+
+        routed_ref[:, c * cw : (c + 1) * cw] = acc[...].astype(BF16)
+
+    def own_first():
+        for load in loads:
+            load.wait()
+        answer(z, 0, 0)
+
+    def near_first():
+        def one(side, c):
+            s = z + 2 * side - 1
+
+            @pl.when(valid(s))
+            def _():
+                arrive(s)
+                answer(s, 0, 0)
+
+            return c
+
+        lax.fori_loop(0, 2, one, 0)
+
+    def near_hidden():
+        for j in range(2 * nc):
+            from_core(j)
+
+        def one(side, c):
+            s = z + 2 * side - 1
+
+            @pl.when(valid(s))
+            def _():
+                hidden(s, 1, side)
+
+            return c
+
+        lax.fori_loop(0, 2, one, 0)
+
+    def near_down(c):
+        from_core(2 * nc + c)
+
+        def one(side, carry):
+            s = z + 2 * side - 1
+
+            @pl.when(valid(s))
+            def _():
+                down(s, 1, side, c, share(s, 1))
+
+                @pl.when(at_end(s))
+                def _():
+                    compact_copy(s, 1, c).start()
+
+            return carry
+
+        lax.fori_loop(0, 2, one, 0)
+
+    def further(d):
+        def one(i, c):
+            s = z + d * (2 * (i // 2) - 1)
+            e = lax.rem(i, 2)
+
+            @pl.when(valid(s))
+            def _():
+                @pl.when(e == 0)
+                def _():
+                    arrive(s)
+
+                answer(s, e, 0)
+
+            return c
+
+        lax.fori_loop(0, 4, one, 0)
+
+    plan = {j: [] for j in range(pieces + 2)}
+
+    def at(part, what, *args):
+        plan[min(int(part * pieces), pieces + 1)].append((what, args))
+
+    at(0.0, own_first)
+    at(0.09, join_pair)
+    at(0.09, hop, 0)
+    for r in range(nt):
+        at(0.17 + 0.26 * r / nt, attend, r)
+    if groups > 2:
+        for c in range(nc):
+            at((0.42 * c + 0.42) / nc, forward, 0, c)
+    at(0.51, near_first)
+    at(0.51, hop, 1)
+    for i in range(1, groups - 2):
+        for c in range(nc):
+            at(0.59 + 0.34 * c / nc, forward, i, c)
+    for i in range(2, groups - 1):
+        at(0.76, hop, i)
+    at(0.8, near_hidden)
+    for c in range(nc):
+        plan[2 * nc + 2 + c].append((near_down, (c,)))
+
+    for j in range(pieces + 2):
+        if j < pieces:
+            from_partner(j)
+        if j >= 2:
+            from_peers(j - 2)
+        for what, args in plan[j]:
+            what(*args)
+
+    if groups > 2:
+        further(2)
+    if groups > 2:
+        hop(groups - 1)
+    attend_end()
     lax.fori_loop(1, nt, send_part, 0)
     project(tp)
-
-    lax.fori_loop(1, groups - 1, serve, 0)
-
-    def give_back(j, c):
-        s, valid = where_is(2 * (groups - 1) - 1 - j)
-
-        @pl.when(valid & jnp.logical_not(at_end(s)))
-        def _():
-            mine = combined(s)
-            ret_copy(s, s, grp).wait_recv()
-            part[s] = (mine + ret[s].astype(F32)).astype(BF16)
-            hop(s).start()
-
-        return c
-
-    lax.fori_loop(0, 2 * (groups - 1), give_back, 0)
-
-    def mix(i, total):
-        j = lax.rem(tp + i, nt)
-        part_arrival(j).wait_recv()
-        return total + prec[j].astype(F32)
-
-    projected = pout[tp].astype(F32)
-    for i in range(1, nt):
-        projected = mix(i, projected)
-    mixed_ref[...] = rms(projected, ps_ref[...]).astype(BF16)
-
-    acc[...] = combined(grp)
-    for slot, there in ((grp, grp + 1 < groups), (groups, grp > 0)):
-        @pl.when(there)
-        def _():
-            ret_copy(grp, slot, grp).wait_recv()
-            acc[...] += ret[slot].astype(F32)
-
-    routed_ref[...] = acc[...].astype(BF16)
-
-    def finish(s, c):
-        swap_copy(0, s).wait_send()
-        swap_copy(1, s).wait_send()
-
-        @pl.when(s != grp)
-        def _():
-            hop(s).wait_send()
-            info_copy(s, grp).wait_send()
-
-        for h in range(2):
-            @pl.when((s != grp) & jnp.logical_not(at_end(s)))
+    answer(z, 1, 0)
+    for d in range(3, groups):
+        further(d)
+
+    for turn in range(1, groups):
+        low, high = groups - 1 - turn, turn
+        for t in range(nc + max(groups - 3, 0)):
+            for h in range(1, min(turn, groups - 1)):
+                c = t - (h - 1)
+                if 0 <= c < nc:
+                    @pl.when(z == groups - 1 - h)
+                    def _():
+                        pass_on(low, c)
+
+                    @pl.when(z == h)
+                    def _():
+                        pass_on(high, c)
+
+            if t < nc and turn >= 2:
+                @pl.when(jnp.maximum(z, groups - 1 - z) == turn - 1)
+                def _():
+                    own_end(t)
+
+            if turn == groups - 1 and t == 2:
+                mix()
+
+    for c in range(nc):
+        @pl.when(jnp.maximum(z, groups - 1 - z) == groups - 1)
+        def _():
+            own_end(c)
+
+    for j in range(pieces):
+        x_copy(j).wait_send()
+        core_copy(tp, j).wait_send()
+        for o in range(1, nt // 2):
+            y_copy(o, j).wait_send()
+            core_copy(lax.rem(tp + 2 * o, nt), j).wait_send()
+    for copy in pair_copies(par):
+        copy.wait_send()
+
+    @pl.when(z + 1 < groups)
+    def _():
+        for copy in pre_copies():
+            copy.wait_send()
+
+    def finish(s, carry):
+        for c in range(nc):
+            @pl.when((s <= z) & (z + 1 < groups))
             def _():
-                tok_copy(s, h, grp, s).wait_send()
-
-        return c
+                tok_copy(1, s, c).wait_send()
+
+            @pl.when((s >= z) & (z > 0))
+            def _():
+                tok_copy(0, s, c).wait_send()
+
+        @pl.when(s != z)
+        def _():
+            info_copy(s, z).wait_send()
+
+            @pl.when(at_end(s))
+            def _():
+                for e in range(2):
+                    for c in range(nc):
+                        compact_copy(s, e, c).wait_send()
+
+            @pl.when(jnp.logical_not(at_end(s)))
+            def _():
+                for c in range(nc):
+                    sum_copy(s, c).wait_send()
+
+        return carry
 
     lax.fori_loop(0, groups, finish, 0)
-    for h in range(2):
-        @pl.when(grp + 1 < groups)
-        def _():
-            tok_copy(grp, h, grp, grp).wait_send()
-
-        @pl.when(grp > 0)
-        def _():
-            tok_copy(grp, h, grp, groups).wait_send()
-
-    def finish_group(g, c):
-        for copy in group_copies(g):
-            copy.wait_send()
-        return c
-
-    lax.fori_loop(grp + 1, groups, finish_group, 0)
     for i in range(1, nt):
         part_copy(lax.rem(tp + i, nt)).wait_send()
 
@@ -765,30 +936,79 @@
     dma = pltpu.SemaphoreType.DMA
     slots = pltpu.VMEM((n, cap, width), BF16)
     groups = n // 2
-    relay = groups * tokens * width * 6 < 24 * 1024 * 1024
+    nc = 4
+    cw = width // nc
     wide = -(-tokens // 128) * 128
-    some = pltpu.VMEM((groups, cap, width), BF16)
-    if relay:
-        body = relay_kernel
-        buffers = [
-            pltpu.VMEM((groups, tokens, width), BF16),
-            pltpu.VMEM((groups, 8, wide), F32),
-            some, some, some, some, some,
-            pltpu.VMEM((groups, tokens, width), BF16),
-            pltpu.VMEM((groups + 1, tokens, width), BF16),
-            pltpu.VMEM((tokens, width), F32),
-        ]
-        sems = [dma((groups + 1, 2)), dma((groups, 2))] + [dma((groups,))] * 7 + [dma((groups + 1,))]
-    else:
-        body = kernel
-        buffers = [
-            slots, slots, slots, slots,
-            pltpu.VMEM((tokens, width), BF16),
-            pltpu.VMEM((tokens, width), F32),
-        ]
-        sems = [dma((n,))] * 4
+    near = groups * tokens * width * 6 < 24 * 1024 * 1024 and nt % 2 == 0
+    if near:
+        pair_w = (2, width, hidden)
+        pieces = 3 * nc
+        slot = (groups, nc, 2 * cap, cw)
+        slot_in = (groups + 1, nc, 2 * cap, cw)
+        line = (groups, nc, tokens, cw)
+        line_in = (groups + 1, nc, tokens, cw)
+        return pl.pallas_call(
+            functools.partial(plane_kernel, n, nt, cap, nc),
+            out_shape=(
+                jax.ShapeDtypeStruct((rows, width), BF16),
+                jax.ShapeDtypeStruct((tokens, width), BF16),
+            ),
+            in_specs=[vm] * 7 + [hbm] + [vm] * 6 + [hbm] * 3,
+            out_specs=(vm, vm),
+            scratch_shapes=[
+                pltpu.VMEM(pair_w, BF16),
+                pltpu.VMEM(pair_w, BF16),
+                pltpu.VMEM((2, hidden, width), BF16),
+                pltpu.VMEM((hd, width), BF16),
+                pltpu.VMEM(line, BF16),
+                pltpu.VMEM((groups, 8, wide), F32),
+                pltpu.VMEM((cap, width), BF16),
+                pltpu.VMEM((2, cap, hidden), BF16),
+                pltpu.VMEM(slot, BF16),
+                pltpu.VMEM(slot_in, BF16),
+                pltpu.VMEM(line, BF16),
+                pltpu.VMEM(line_in, BF16),
+                pltpu.VMEM((tokens, cw), F32),
+                pltpu.VMEM((2, hd, hd), BF16),
+                pltpu.VMEM((2, 8, hd), F32),
+                pltpu.VMEM((hd, hd), F32),
+                pltpu.VMEM((8, hd), F32),
+                pltpu.VMEM((2, hd, hd), BF16),
+                pltpu.VMEM((2, 8, hd), F32),
+                pltpu.VMEM((hd, hd), F32),
+                pltpu.VMEM((length, hd), F32),
+                pltpu.VMEM((length, 128), F32),
+                pltpu.VMEM((length, hd), BF16),
+                pltpu.VMEM((nt, rows, width), BF16),
+                pltpu.VMEM((nt, rows, width), BF16),
+                dma((4,)),
+                dma((pieces,)), dma((nt // 2, pieces)), dma((nt // 2, pieces)), dma((nt, pieces)),
+                dma((2, groups, nc)), dma((groups, nc)),
+                dma((groups,)), dma((groups,)),
+                dma((groups, 2, nc)), dma((groups + 1, 2, nc)),
+                dma((groups, nc)), dma((groups + 1, nc)),
+                dma, dma, dma, dma, dma, dma, dma, dma,
+                dma((nt,)), dma((nt,)),
+            ],
+            compiler_params=pltpu.CompilerParams(
+                collective_id=0, has_side_effects=True, vmem_limit_bytes=62 * 1024 * 1024
+            ),
+        )(
+            memory_query_matrix, memory_key_matrix, memory_value_matrix,
+            input_gate_logits, forget_gate_logits, forget_log_boosts,
+            head_norm_scale[None], memory_output_matrix, projection_norm_scale[None],
+            second_batch_rows, expert_prenorm_scale[None], selected_expert_index.T,
+            group_route_probability[None], expert_choice_scores.T,
+            expert_gate_matrix, expert_up_matrix, expert_down_matrix,
+        )
+    buffers = [
+        slots, slots, slots, slots,
+        pltpu.VMEM((tokens, width), BF16),
+        pltpu.VMEM((tokens, width), F32),
+    ]
+    sems = [dma((n,))] * 4
     return pl.pallas_call(
-        functools.partial(body, n, nt, cap),
+        functools.partial(kernel, n, nt, cap),
         out_shape=(
             jax.ShapeDtypeStruct((rows, width), BF16),
             jax.ShapeDtypeStruct((tokens, width), BF16),

time: 151 us -> 118 us (0.78)
  Pallas kernels: 141 us -> 113 us
  local copies, waits for them, and re-layouts: 8.3 us -> 3.97 us
    pallas_call x1, Pallas kernels: 141 us -> 113 us  [shards(): pl.pallas_call(functools.partial(plane_kernel, n, nt, cap, nc), out_shape...]
    unnamed x4 -> x2, local copies, waits for them, and re-layouts: 6.86 us -> 3.97 us
where the time goes in v1:
time: 118 us; the launch traced here: 117 us
  Pallas kernels  113 us (96%)
  local copies, waits for them, and re-layouts  3.97 us (3%)
    pallas_call x1, Pallas kernels, shards(): pl.pallas_call(functools.partial(plane_kernel, n, nt, cap, nc), out_shape...  113 us
    unnamed x2, local copies, waits for them, and re-layouts  3.97 us

profile of v1, /device:TPU:0, one launch (start us, length us, event | category | flops | bytes accessed | tf_op | source)
XLA Modules:
  0.0 117.4 jit_solution(18110914743555549822)
XLA Ops:
  0.6 112.8 %shard_map.176 = (bf16[128,2048]{1,0:T(8,128)(2,1)}, bf16[192,2048]{1,0:T(8,128)(2,1)}) custom-call(bf16[512,256]{1,0:T(8,128)(2,1)} %q_ref.1, bf16[512,256]{1,0:T(8,128)(2,1)} %k_ref.1, bf16[512,256]{1,0:T(8,128)(2,1)} %v_ref.1, f32[1,512]{1,0:T(1,128)} %ig_ref.1, f32[1,512]{1,0:T(1,128)} %fg_ref.1, f32[1,512]{1,0:T(1,128)} %fb_ref.1, f32[1,256]{1,0:T(1,128)} %bitcast.10, ...), custom_call_target="tpu_custom_call" | custom-call | tf_op jit(solution)/shard_map/pallas_call | solution.py:950
  113.4 1.9 %copy.21 = bf16[128,2048]{1,0:T(8,128)(2,1)} copy(bf16[128,2048]{1,0:T(8,128)(2,1)} %get-tuple-element.4) | data formatting | bytes 1048576
  115.3 2.1 %copy.22 = bf16[192,2048]{1,0:T(8,128)(2,1)} copy(bf16[192,2048]{1,0:T(8,128)(2,1)} %get-tuple-element.5) | data formatting | bytes 1572864

commit v2 on v1

--- a/solution.py
+++ b/solution.py
@@ -331,13 +331,13 @@
 
 
 def plane_kernel(
-    n, nt, cap, nc,
+    n, nt, cap, nc, wc,
     q_ref, k_ref, v_ref, ig_ref, fg_ref, fb_ref, hs_ref, wo_hbm, ps_ref,
     x_ref, es_ref, ids_ref, grp_ref, sc_ref, wg_hbm, wu_hbm, wd_hbm,
     mixed_ref, routed_ref,
     wg, wu, wd, wo, tok, info, chosen, hid, ans, cin, rout, rin, acc,
     cpair, spair, cgrp, sgrp, cpre, spre, ent, num, stat, head, pout, prec,
-    wsem, x_ss, y_ss, k_ss, w_rs, t_ss, t_rs, i_ss, i_rs, c_ss, c_rs, r_ss, r_rs,
+    wsem, x_ss, y_ss, k_ss, w_rs, t_ss, t_rs, i_ss, i_rs, c_ss, r_ss, r_rs,
     c1s, c1r, s1s, s1r, c2s, c2r, s2s, s2r, p_ss, p_rs,
 ):
     me = lax.axis_index("ep")
@@ -351,7 +351,7 @@
     length, hd = q_ref.shape
     rows = mixed_ref.shape[0]
     cw = width // nc
-    pieces = 3 * nc
+    pieces = 3 * wc
 
     def remote(src, dst, ss, rs, to):
         return pltpu.make_async_remote_copy(
@@ -377,32 +377,37 @@
         load.start()
 
     def piece(ref, lead, part, j):
-        which, at = divmod(j, nc)
+        which, at = divmod(j, wc)
         if which < 2:
             quarter = ref[which].shape[1] // nt
-            step = quarter // nc
+            step = quarter // wc
             return ref[which].at[lead, pl.ds(pl.multiple_of(part * quarter + at * step, step), step)]
         quarter = ref[2].shape[1] // nt
-        step = width // nc
+        step = width // wc
         return ref[2].at[lead, pl.ds(pl.multiple_of(part * quarter, quarter), quarter), pl.ds(at * step, step)]
 
     held = (wg, wu, wd)
     given = (wg_hbm, wu_hbm, wd_hbm)
 
     def x_copy(j):
-        return remote(piece(given, 0, tp, j), piece(held, 1, tp, j), x_ss.at[j], w_rs.at[tp, j], (partner, tp))
+        return remote(piece(given, 0, tp, j), piece(held, 1, tp, j), x_ss.at[j // wc], w_rs.at[tp, j], (partner, tp))
 
     def y_copy(o, j):
         here = piece(held, 1, tp, j)
-        return remote(here, here, y_ss.at[o, j], w_rs.at[tp, j], (me, lax.rem(tp + 2 * o, nt)))
+        return remote(here, here, y_ss.at[o, j // wc], w_rs.at[tp, j], (me, lax.rem(tp + 2 * o, nt)))
 
     def core_copy(part, j):
         here = piece(held, 1, part, j)
-        return remote(here, here, k_ss.at[part // 2, j], w_rs.at[part, j], (me, other))
+        sem = w_rs.at[part, j // wc * wc if j < 2 * wc else j]
+        return remote(here, here, k_ss.at[part // 2, j // wc], sem, (me, other))
 
     def weight_wait(part, j):
         here = piece(held, 1, part, j)
-        remote(here, here, x_ss.at[j], w_rs.at[part, j], (me, other)).wait_recv()
+        remote(here, here, x_ss.at[j // wc], w_rs.at[part, j], (me, other)).wait_recv()
+
+    def quarter(which, part):
+        step = held[which].shape[1] // nt
+        return held[which].at[1, pl.ds(pl.multiple_of(part * step, step), step)]
 
     def from_partner(j):
         weight_wait(tp, j)
@@ -418,15 +423,20 @@
 
     def from_core(j):
         for o in range(nt // 2):
-            weight_wait(lax.rem(other + 2 * o, nt), j)
+            part = lax.rem(other + 2 * o, nt)
+            if j < 2 * wc:
+                here = quarter(j // wc, part)
+                remote(here, here, x_ss.at[0], w_rs.at[part, j], (me, other)).wait_recv()
+            else:
+                weight_wait(part, j)
 
     def tok_copy(up, s, c):
         here = tok.at[s, c]
-        return remote(here, here, t_ss.at[up, s, c], t_rs.at[s, c], ((z - 1 + 2 * up) * 2 + par, tp))
+        return remote(here, here, t_ss.at[up, s], t_rs.at[s, c], ((z - 1 + 2 * up) * 2 + par, tp))
 
     def tok_wait(s, c):
         here = tok.at[s, c]
-        remote(here, here, t_ss.at[0, s, c], t_rs.at[s, c], (me, other)).wait_recv()
+        remote(here, here, t_ss.at[0, s], t_rs.at[s, c], (me, other)).wait_recv()
 
     def send_own(c):
         @pl.when(z + 1 < groups)
@@ -437,23 +447,49 @@
         def _():
             tok_copy(0, z, c).start()
 
-    def forward(i, c):
-        @pl.when((z - 1 - i >= 0) & (z + 1 < groups))
-        def _():
-            tok_wait(z - 1 - i, c)
-            tok_copy(1, z - 1 - i, c).start()
-
-        @pl.when((z + 1 + i < groups) & (z > 0))
-        def _():
-            tok_wait(z + 1 + i, c)
-            tok_copy(0, z + 1 + i, c).start()
+    def near_arrive(c):
+        @pl.when(z > 0)
+        def _():
+            tok_wait(z - 1, c)
+
+            @pl.when((z == 1) & (z + 1 < groups))
+            def _():
+                tok_copy(1, z - 1, c).start()
+
+        @pl.when(z + 1 < groups)
+        def _():
+            tok_wait(z + 1, c)
+
+            @pl.when((z == groups - 2) & (z > 0))
+            def _():
+                tok_copy(0, z + 1, c).start()
+
+    def near_forward(c):
+        @pl.when((z >= 2) & (z + 1 < groups))
+        def _():
+            tok_copy(1, z - 1, c).start()
+
+        @pl.when((z <= groups - 3) & (z > 0))
+        def _():
+            tok_copy(0, z + 1, c).start()
+
+    def far_forward(i, c):
+        @pl.when((i < z) & (z + 1 < groups))
+        def _():
+            tok_wait(i - 1, c)
+            tok_copy(1, i - 1, c).start()
+
+        @pl.when((i < groups - 1 - z) & (z > 0))
+        def _():
+            tok_wait(groups - i, c)
+            tok_copy(0, groups - i, c).start()
 
     normed = rms(x_ref[...].astype(F32), es_ref[...]).astype(BF16)
     for c in range(nc):
         tok[z, c] = normed[:, c * cw : (c + 1) * cw]
 
     pl.semaphore_wait(barrier, n - 1 + nt - 1)
-    early = nc // 2
+    early = 5 * nc // 8
     for c in range(early):
         send_own(c)
     for j in range(2):
@@ -522,8 +558,9 @@
         copy.start()
     for j in range(2, pieces):
         x_copy(j).start()
-    for c in range(early, nc):
-        send_own(c)
+    def send_rest():
+        for c in range(early, nc):
+            send_own(c)
 
     def pre_copies():
         to = ((z + 1) * 2 + par, tp)
@@ -608,6 +645,10 @@
         part_copy(j).start()
         return c
 
+    def send_parts():
+        lax.fori_loop(1, nt, send_part, 0)
+        project(tp)
+
     def mix():
         total = pout[tp].astype(F32)
         for i in range(1, nt):
@@ -653,19 +694,17 @@
     def compact_copy(s, e, c):
         _, to, slot = ret_to(s)
         half = half_of(e)
-        return remote(ans.at[s, c, half], cin.at[slot, c, half], c_ss.at[s, e, c], c_rs.at[slot, e, c], (to * 2 + par, tp))
+        return remote(ans.at[s, c, half], cin.at[slot, c, half], c_ss.at[s], r_rs.at[slot, c], (to * 2 + par, tp))
 
     def compact_wait(slot, c):
-        for e in range(2):
-            half = half_of(e)
-            remote(ans.at[0, c, half], cin.at[slot, c, half], c_ss.at[0, e, c], c_rs.at[slot, e, c], (me, other)).wait_recv()
+        remote(ans.at[0, c], cin.at[slot, c], c_ss.at[0], r_rs.at[slot, c], (me, other)).wait_recv()
 
     def sum_copy(s, c):
         _, to, slot = ret_to(s)
-        return remote(rout.at[s, c], rin.at[slot, c], r_ss.at[s, c], r_rs.at[slot, c], (to * 2 + par, tp))
+        return remote(rout.at[s, c], rin.at[slot, c], r_ss.at[s], r_rs.at[slot, c], (to * 2 + par, tp))
 
     def sum_wait(slot, c):
-        remote(rout.at[0, c], rin.at[slot, c], r_ss.at[0, c], r_rs.at[slot, c], (me, other)).wait_recv()
+        remote(rout.at[0, c], rin.at[slot, c], r_ss.at[0], r_rs.at[slot, c], (me, other)).wait_recv()
 
     def at_end(s):
         return jnp.where(s < z, z == groups - 1, z == 0)
@@ -673,11 +712,12 @@
     def valid(s):
         return (s >= 0) & (s < groups)
 
-    def arrive(s):
-        @pl.when(at_end(s))
-        def _():
-            for c in range(nc):
-                tok_wait(s, c)
+    def arrive(s, rows_too):
+        if rows_too:
+            @pl.when(at_end(s))
+            def _():
+                for c in range(nc):
+                    tok_wait(s, c)
 
         remote(info.at[s], info.at[s], i_ss.at[0], i_rs.at[s], (me, other)).wait_recv()
 
@@ -730,7 +770,7 @@
         def _():
             upstream(z, groups, z - 1, 0, c, put)
 
-        routed_ref[:, c * cw : (c + 1) * cw] = acc[...].astype(BF16)
+        routed_ref[:, pl.ds(pl.multiple_of(c * cw, cw), cw)] = acc[...].astype(BF16)
 
     def own_first():
         for load in loads:
@@ -743,7 +783,7 @@
 
             @pl.when(valid(s))
             def _():
-                arrive(s)
+                arrive(s, False)
                 answer(s, 0, 0)
 
             return c
@@ -751,7 +791,7 @@
         lax.fori_loop(0, 2, one, 0)
 
     def near_hidden():
-        for j in range(2 * nc):
+        for j in (0, wc):
             from_core(j)
 
         def one(side, c):
@@ -766,7 +806,8 @@
         lax.fori_loop(0, 2, one, 0)
 
     def near_down(c):
-        from_core(2 * nc + c)
+        if c % (nc // wc) == 0:
+            from_core(2 * wc + c * wc // nc)
 
         def one(side, carry):
             s = z + 2 * side - 1
@@ -784,45 +825,65 @@
         lax.fori_loop(0, 2, one, 0)
 
     def further(d):
-        def one(i, c):
-            s = z + d * (2 * (i // 2) - 1)
-            e = lax.rem(i, 2)
+        def one(side, carry):
+            s = z + d * (2 * side - 1)
 
             @pl.when(valid(s))
             def _():
-                @pl.when(e == 0)
-                def _():
-                    arrive(s)
-
-                answer(s, e, 0)
-
-            return c
-
-        lax.fori_loop(0, 4, one, 0)
+                arrive(s, True)
+
+                def first(e, c):
+                    hidden(s, e, e)
+                    return c
+
+                lax.fori_loop(0, 2, first, 0)
+                weights = [share(s, e) for e in range(2)]
+                for c in range(nc):
+                    for e in range(2):
+                        down(s, e, e, c, weights[e])
+
+                        @pl.when(at_end(s))
+                        def _():
+                            compact_copy(s, e, c).start()
+
+            return carry
+
+        lax.fori_loop(0, 2, one, 0)
 
     plan = {j: [] for j in range(pieces + 2)}
 
     def at(part, what, *args):
-        plan[min(int(part * pieces), pieces + 1)].append((what, args))
-
-    at(0.0, own_first)
-    at(0.09, join_pair)
-    at(0.09, hop, 0)
+        plan[min(int(part * pieces / 12), pieces + 1)].append((what, args))
+
+    def spread(start, end, what, *args, chunks=range(nc)):
+        for c in chunks:
+            at(start + (end - start) * c / nc, what, *args, c)
+
+    at(0, own_first)
+    at(1, join_pair)
+    at(1, hop, 0)
+    at(1, send_rest)
     for r in range(nt):
-        at(0.17 + 0.26 * r / nt, attend, r)
-    if groups > 2:
-        for c in range(nc):
-            at((0.42 * c + 0.42) / nc, forward, 0, c)
-    at(0.51, near_first)
-    at(0.51, hop, 1)
+        at(2 + 2 * r / nt, attend, r)
+    at(3, hop, 1)
+    at(3, near_arrive, 0)
+    spread(3, 5, near_arrive, chunks=range(1, nc))
+    lead = nc // 4
+    if groups > 3:
+        spread(4, 4, near_forward, chunks=range(lead))
+    for i in range(2, groups - 1):
+        at(5, hop, i)
+    at(5, near_first)
     for i in range(1, groups - 2):
-        for c in range(nc):
-            at(0.59 + 0.34 * c / nc, forward, i, c)
-    for i in range(2, groups - 1):
-        at(0.76, hop, i)
-    at(0.8, near_hidden)
+        spread(6.3, 11.9, far_forward, i)
+    if groups > 3:
+        spread(11, 11, near_forward, chunks=range(lead, nc))
+    at(8, hop, groups - 1)
+    at(8, attend_end)
+    at(9, near_hidden)
     for c in range(nc):
-        plan[2 * nc + 2 + c].append((near_down, (c,)))
+        at(10 + 4 * c / nc, near_down, c)
+    at(12, send_parts)
 
     for j in range(pieces + 2):
         if j < pieces:
@@ -832,50 +893,63 @@
         for what, args in plan[j]:
             what(*args)
 
-    if groups > 2:
-        further(2)
-    if groups > 2:
-        hop(groups - 1)
-    attend_end()
-    lax.fori_loop(1, nt, send_part, 0)
-    project(tp)
-    answer(z, 1, 0)
-    for d in range(3, groups):
+    turns = [1, *range(groups - 1, 1, -1)]
+    lag = 3
+    further(turns[1])
+
+    @pl.when((z == 0) | (z == groups - 1))
+    def _():
+        answer(z, 1, 0)
+
+    for d in turns[2:]:
         further(d)
 
-    for turn in range(1, groups):
-        low, high = groups - 1 - turn, turn
-        for t in range(nc + max(groups - 3, 0)):
+    def last_turn(g):
+        return max(turns.index(t) for t in (g, groups - 1 - g) if t)
+
+    def events(t, carry):
+        def during(start, what, *args):
+            c = t - start
+
+            @pl.when((c >= 0) & (c < nc))
+            def _():
+                what(*args, c)
+
+        for step, turn in enumerate(turns[1:]):
             for h in range(1, min(turn, groups - 1)):
-                c = t - (h - 1)
-                if 0 <= c < nc:
-                    @pl.when(z == groups - 1 - h)
-                    def _():
-                        pass_on(low, c)
-
-                    @pl.when(z == h)
-                    def _():
-                        pass_on(high, c)
-
-            if t < nc and turn >= 2:
-                @pl.when(jnp.maximum(z, groups - 1 - z) == turn - 1)
+                @pl.when(z == groups - 1 - h)
                 def _():
-                    own_end(t)
-
-            if turn == groups - 1 and t == 2:
-                mix()
-
-    for c in range(nc):
-        @pl.when(jnp.maximum(z, groups - 1 - z) == groups - 1)
-        def _():
-            own_end(c)
-
-    for j in range(pieces):
-        x_copy(j).wait_send()
-        core_copy(tp, j).wait_send()
-        for o in range(1, nt // 2):
-            y_copy(o, j).wait_send()
-            core_copy(lax.rem(tp + 2 * o, nt), j).wait_send()
+                    during(step * nc + lag * (h - 1), pass_on, groups - 1 - turn)
+
+                @pl.when(z == h)
+                def _():
+                    during(step * nc + lag * (h - 1), pass_on, turn)
+
+        @pl.when(t == 3)
+        def _():
+            @pl.when((z > 0) & (z < groups - 1))
+            def _():
+                answer(z, 1, 0)
+
+        @pl.when(t == nc + 2)
+        def _():
+            mix()
+
+        closing = jnp.int32(0)
+        for g in range(groups):
+            closing = jnp.where(z == g, (last_turn(g) - 1) * nc + lag * max(groups - 3, 1), closing)
+        during(closing, own_end)
+        return carry
+
+    lax.fori_loop(0, max(groups - 2, 1) * nc + lag * max(groups - 3, 1), events, 0)
+
+    for which in range(3):
+        here = quarter(which, tp)
+        remote(here, here, x_ss.at[which], w_rs.at[0, 0], (partner, tp)).wait_send()
+        for o in range(nt // 2):
+            if o:
+                remote(here, here, y_ss.at[o, which], w_rs.at[0, 0], (partner, tp)).wait_send()
+            remote(here, here, k_ss.at[o, which], w_rs.at[0, 0], (me, other)).wait_send()
     for copy in pair_copies(par):
         copy.wait_send()
 
@@ -884,15 +958,17 @@
         for copy in pre_copies():
             copy.wait_send()
 
+    def sent(ref, sem):
+        remote(ref, ref, sem, t_rs.at[0, 0], (me, other)).wait_send()
+
     def finish(s, carry):
-        for c in range(nc):
-            @pl.when((s <= z) & (z + 1 < groups))
-            def _():
-                tok_copy(1, s, c).wait_send()
-
-            @pl.when((s >= z) & (z > 0))
-            def _():
-                tok_copy(0, s, c).wait_send()
+        @pl.when((s <= z) & (z + 1 < groups))
+        def _():
+            sent(tok.at[s], t_ss.at[1, s])
+
+        @pl.when((s >= z) & (z > 0))
+        def _():
+            sent(tok.at[s], t_ss.at[0, s])
 
         @pl.when(s != z)
         def _():
@@ -900,14 +976,11 @@
 
             @pl.when(at_end(s))
             def _():
-                for e in range(2):
-                    for c in range(nc):
-                        compact_copy(s, e, c).wait_send()
+                sent(ans.at[s], c_ss.at[s])
 
             @pl.when(jnp.logical_not(at_end(s)))
             def _():
-                for c in range(nc):
-                    sum_copy(s, c).wait_send()
+                sent(rout.at[s], r_ss.at[s])
 
         return carry
 
@@ -936,19 +1009,19 @@
     dma = pltpu.SemaphoreType.DMA
     slots = pltpu.VMEM((n, cap, width), BF16)
     groups = n // 2
-    nc = 4
+    nc, wc = 8, 4
     cw = width // nc
     wide = -(-tokens // 128) * 128
-    near = groups * tokens * width * 6 < 24 * 1024 * 1024 and nt % 2 == 0
+    near = groups * tokens * width * 6 < 24 * 1024 * 1024 and nt % 2 == 0 and groups > 3
     if near:
         pair_w = (2, width, hidden)
-        pieces = 3 * nc
+        pieces = 3 * wc
         slot = (groups, nc, 2 * cap, cw)
         slot_in = (groups + 1, nc, 2 * cap, cw)
         line = (groups, nc, tokens, cw)
         line_in = (groups + 1, nc, tokens, cw)
         return pl.pallas_call(
-            functools.partial(plane_kernel, n, nt, cap, nc),
+            functools.partial(plane_kernel, n, nt, cap, nc, wc),
             out_shape=(
                 jax.ShapeDtypeStruct((rows, width), BF16),
                 jax.ShapeDtypeStruct((tokens, width), BF16),
@@ -982,11 +1055,10 @@
                 pltpu.VMEM((nt, rows, width), BF16),
                 pltpu.VMEM((nt, rows, width), BF16),
                 dma((4,)),
-                dma((pieces,)), dma((nt // 2, pieces)), dma((nt // 2, pieces)), dma((nt, pieces)),
-                dma((2, groups, nc)), dma((groups, nc)),
+                dma((3,)), dma((nt // 2, 3)), dma((nt // 2, 3)), dma((nt, pieces)),
+                dma((2, groups)), dma((groups, nc)),
                 dma((groups,)), dma((groups,)),
-                dma((groups, 2, nc)), dma((groups + 1, 2, nc)),
-                dma((groups, nc)), dma((groups + 1, nc)),
+                dma((groups,)), dma((groups,)), dma((groups + 1, nc)),
                 dma, dma, dma, dma, dma, dma, dma, dma,
                 dma((nt,)), dma((nt,)),
             ],

time: 118 us -> 104 us (0.88)
  the two profiles are of different devices: /device:TPU:0 before, /device:TPU:9 now
where the time goes in v2:
time: 104 us
  Pallas kernels  99 us (95%)
  local copies, waits for them, and re-layouts  3.97 us (4%)
    pallas_call x1, Pallas kernels, shards(): pl.pallas_call(functools.partial(plane_kernel, n, nt, cap, nc, wc), out_s...  99 us
    unnamed x2, local copies, waits for them, and re-layouts  3.97 us

profile of v2, /device:TPU:9, one launch (start us, length us, event | category | flops | bytes accessed | tf_op | source)
XLA Modules:
  0.0 103.6 jit_solution(16044359709657989649)
XLA Ops:
  0.6 99.0 %shard_map.176 = (bf16[128,2048]{1,0:T(8,128)(2,1)}, bf16[192,2048]{1,0:T(8,128)(2,1)}) custom-call(bf16[512,256]{1,0:T(8,128)(2,1)} %q_ref.1, bf16[512,256]{1,0:T(8,128)(2,1)} %k_ref.1, bf16[512,256]{1,0:T(8,128)(2,1)} %v_ref.1, f32[1,512]{1,0:T(1,128)} %ig_ref.1, f32[1,512]{1,0:T(1,128)} %fg_ref.1, f32[1,512]{1,0:T(1,128)} %fb_ref.1, f32[1,256]{1,0:T(1,128)} %bitcast.10, ...), custom_call_target="tpu_custom_call" | custom-call | tf_op jit(solution)/shard_map/pallas_call | solution.py:1023
  99.7 1.9 %copy.21 = bf16[128,2048]{1,0:T(8,128)(2,1)} copy(bf16[128,2048]{1,0:T(8,128)(2,1)} %get-tuple-element.4) | data formatting | bytes 1048576
  101.5 2.1 %copy.22 = bf16[192,2048]{1,0:T(8,128)(2,1)} copy(bf16[192,2048]{1,0:T(8,128)(2,1)} %get-tuple-element.5) | data formatting | bytes 1572864

commit v3 on v2

--- a/solution.py
+++ b/solution.py
@@ -335,7 +335,7 @@
     q_ref, k_ref, v_ref, ig_ref, fg_ref, fb_ref, hs_ref, wo_hbm, ps_ref,
     x_ref, es_ref, ids_ref, grp_ref, sc_ref, wg_hbm, wu_hbm, wd_hbm,
     mixed_ref, routed_ref,
-    wg, wu, wd, wo, tok, info, chosen, hid, ans, cin, rout, rin, acc,
+    wg, wu, wd, wo, tok, info, chosen, hid, ans, cin, rout, rin, acc, gu,
     cpair, spair, cgrp, sgrp, cpre, spre, ent, num, stat, head, pout, prec,
     wsem, x_ss, y_ss, k_ss, w_rs, t_ss, t_rs, i_ss, i_rs, c_ss, r_ss, r_rs,
     c1s, c1r, s1s, s1r, c2s, c2r, s2s, s2r, p_ss, p_rs,
@@ -724,12 +724,14 @@
     def answer(s, e, at):
         hidden(s, e, at)
         weight = share(s, e)
-        for c in range(nc):
-            down(s, e, at, c, weight)
+        for g in range(wc):
+            for c in group(g):
+                down(s, e, at, c, weight)
 
             @pl.when((s != z) & at_end(s))
             def _():
-                compact_copy(s, e, c).start()
+                for c in group(g):
+                    compact_copy(s, e, c).start()
 
     def scatter(s, plane, block):
         is_a, is_b, _, _ = masks(s, plane, 0, 2 * cap)
@@ -805,30 +807,88 @@
 
         lax.fori_loop(0, 2, one, 0)
 
-    def near_down(c):
-        if c % (nc // wc) == 0:
-            from_core(2 * wc + c * wc // nc)
+    def near_send(s, g):
+        @pl.when(valid(s) & at_end(s))
+        def _():
+            for c in group(g):
+                compact_copy(s, 1, c).start()
+
+    def near_down(g):
+        from_core(2 * wc + g)
 
         def one(side, carry):
             s = z + 2 * side - 1
 
             @pl.when(valid(s))
             def _():
-                down(s, 1, side, c, share(s, 1))
-
-                @pl.when(at_end(s))
-                def _():
-                    compact_copy(s, 1, c).start()
+                weight = share(s, 1)
+                for c in group(g):
+                    down(s, 1, side, c, weight)
+
+                if g < wc - 1:
+                    near_send(s, g)
 
             return carry
 
         lax.fori_loop(0, 2, one, 0)
+
+    def group(g):
+        return range(g * (nc // wc), (g + 1) * (nc // wc))
+
+    far = jnp.where(z < groups // 2, groups - 1, 0)
+
+    def far_step(g):
+        size = nc // wc
+        span = slice(g * size * cw, (g + 1) * size * cw)
+
+        @pl.when(at_end(far))
+        def _():
+            for c in group(g):
+                tok_wait(far, c)
+
+        if g == 0:
+            arrive(far, False)
+
+        def one(e, carry):
+            is_a, is_b, _, _ = masks(far, z, e * cap, cap)
+            place = (is_a | is_b).astype(BF16)
+            for c in group(g):
+                chosen[:, c * cw : (c + 1) * cw] = dot(place, tok[far, c]).astype(BF16)
+            for which, ref in enumerate((wg, wu)):
+                part = dot(chosen[:, span], ref[e, span, :])
+                gu[e, which] = part if g == 0 else gu[e, which] + part
+            return carry
+
+        lax.fori_loop(0, 2, one, 0)
+
+    def far_hidden():
+        def one(e, carry):
+            gate = gu[e, 0]
+            hid[2 + e] = (gate / (1.0 + jnp.exp(-gate)) * gu[e, 1]).astype(BF16)
+            return carry
+
+        lax.fori_loop(0, 2, one, 0)
+
+    def both_down(s, at, g):
+        weights = [share(s, e) for e in range(2)]
+        for c in group(g):
+            for e in range(2):
+                down(s, e, at + e, c, weights[e])
+
+        @pl.when(at_end(s))
+        def _():
+            for c in group(g):
+                for e in range(2):
+                    compact_copy(s, e, c).start()
+
+    def far_down(g):
+        both_down(far, 2, g)
 
     def further(d):
         def one(side, carry):
             s = z + d * (2 * side - 1)
 
-            @pl.when(valid(s))
+            @pl.when(valid(s) & (s != far))
             def _():
                 arrive(s, True)
 
@@ -837,14 +897,8 @@
                     return c
 
                 lax.fori_loop(0, 2, first, 0)
-                weights = [share(s, e) for e in range(2)]
-                for c in range(nc):
-                    for e in range(2):
-                        down(s, e, e, c, weights[e])
-
-                        @pl.when(at_end(s))
-                        def _():
-                            compact_copy(s, e, c).start()
+                for g in range(wc):
+                    both_down(s, 0, g)
 
             return carry
 
@@ -860,30 +914,30 @@
             at(start + (end - start) * c / nc, what, *args, c)
 
     at(0, own_first)
+    at(1, send_rest)
     at(1, join_pair)
     at(1, hop, 0)
-    at(1, send_rest)
     for r in range(nt):
         at(2 + 2 * r / nt, attend, r)
-    at(3, hop, 1)
-    at(3, near_arrive, 0)
-    spread(3, 5, near_arrive, chunks=range(1, nc))
-    lead = nc // 4
-    if groups > 3:
-        spread(4, 4, near_forward, chunks=range(lead))
+    spread(3, 5, near_arrive)
+    lead = 3 * nc // 8
+    spread(3, 3, near_forward, chunks=range(lead))
+    at(5, hop, 1)
+    for i in range(1, groups - 2):
+        spread(5.6, 11.2, far_forward, i)
+    at(5, near_first)
     for i in range(2, groups - 1):
-        at(5, hop, i)
-    at(5, near_first)
-    for i in range(1, groups - 2):
-        spread(6.3, 11.9, far_forward, i)
-    if groups > 3:
-        spread(11, 11, near_forward, chunks=range(lead, nc))
-    at(8, hop, groups - 1)
-    at(8, attend_end)
+        at(11, hop, i)
+    spread(11, 11, near_forward, chunks=range(lead, nc))
     at(9, near_hidden)
-    for c in range(nc):
-        at(10 + 4 * c / nc, near_down, c)
-    at(12, send_parts)
+    for g in range(wc - 1):
+        plan[2 * wc + 2 + g].append((near_down, (g,)))
+        at(11, far_step, g)
+    last = pieces + 1
+    plan[last - 1] += [(far_step, (wc - 1,)), (far_hidden, ())]
+    plan[last - 1] += [(far_down, (g,)) for g in range(wc // 2)]
+    plan[last] += [(far_down, (g,)) for g in range(wc // 2, wc - 1)]
+    plan[last] += [(near_down, (wc - 1,)), (far_down, (wc - 1,)), (hop, (groups - 1,))]
 
     for j in range(pieces + 2):
         if j < pieces:
@@ -895,14 +949,18 @@
 
     turns = [1, *range(groups - 1, 1, -1)]
     lag = 3
-    further(turns[1])
 
     @pl.when((z == 0) | (z == groups - 1))
     def _():
+        attend_end()
+        send_parts()
         answer(z, 1, 0)
 
     for d in turns[2:]:
         further(d)
+
+    for s in (z - 1, z + 1):
+        near_send(s, wc - 1)
 
     def last_turn(g):
         return max(turns.index(t) for t in (g, groups - 1 - g) if t)
@@ -925,13 +983,12 @@
                 def _():
                     during(step * nc + lag * (h - 1), pass_on, turn)
 
-        @pl.when(t == 3)
-        def _():
-            @pl.when((z > 0) & (z < groups - 1))
-            def _():
-                answer(z, 1, 0)
-
-        @pl.when(t == nc + 2)
+        @pl.when((z > 0) & (z < groups - 1))
+        def _():
+            for when, what in ((1, attend_end), (2, send_parts), (4, lambda: answer(z, 1, 0))):
+                pl.when(t == when)(what)
+
+        @pl.when(t == nc + 4)
         def _():
             mix()
 
@@ -1023,8 +1080,8 @@
         return pl.pallas_call(
             functools.partial(plane_kernel, n, nt, cap, nc, wc),
             out_shape=(
-                jax.ShapeDtypeStruct((rows, width), BF16),
-                jax.ShapeDtypeStruct((tokens, width), BF16),
+                pltpu.VMEM((rows, width), BF16),
+                pltpu.VMEM((tokens, width), BF16),
             ),
             in_specs=[vm] * 7 + [hbm] + [vm] * 6 + [hbm] * 3,
             out_specs=(vm, vm),
@@ -1036,12 +1093,13 @@
                 pltpu.VMEM(line, BF16),
                 pltpu.VMEM((groups, 8, wide), F32),
                 pltpu.VMEM((cap, width), BF16),
-                pltpu.VMEM((2, cap, hidden), BF16),
+                pltpu.VMEM((4, cap, hidden), BF16),
                 pltpu.VMEM(slot, BF16),
                 pltpu.VMEM(slot_in, BF16),
                 pltpu.VMEM(line, BF16),
                 pltpu.VMEM(line_in, BF16),
                 pltpu.VMEM((tokens, cw), F32),
+                pltpu.VMEM((2, 2, cap, hidden), F32),
                 pltpu.VMEM((2, hd, hd), BF16),
                 pltpu.VMEM((2, 8, hd), F32),
                 pltpu.VMEM((hd, hd), F32),
@@ -1063,7 +1121,7 @@
                 dma((nt,)), dma((nt,)),
             ],
             compiler_params=pltpu.CompilerParams(
-                collective_id=0, has_side_effects=True, vmem_limit_bytes=62 * 1024 * 1024
+                collective_id=0, has_side_effects=True, vmem_limit_bytes=56 * 1024 * 1024
             ),
         )(
             memory_query_matrix, memory_key_matrix, memory_value_matrix,

time: 104 us -> 96.3 us (0.926)
  Pallas kernels: 99 us -> 93.8 us
  local copies, waits for them, and re-layouts: 3.97 us -> 1.67 us
    pallas_call x1, Pallas kernels: 99 us -> 93.8 us  [shards(): pl.pallas_call(functools.partial(plane_kernel, n, nt, cap, nc, wc), out_s...]
    unnamed x2, local copies, waits for them, and re-layouts: 3.97 us -> 1.67 us
where the time goes in v3:
time: 96.3 us; the launch traced here: 96.1 us
  Pallas kernels  93.8 us (97%)
  local copies, waits for them, and re-layouts  1.67 us (2%)
    pallas_call x1, Pallas kernels, shards(): pl.pallas_call(functools.partial(plane_kernel, n, nt, cap, nc, wc), out_s...  93.8 us

profile of v3, /device:TPU:9, one launch (start us, length us, event | category | flops | bytes accessed | tf_op | source)
XLA Modules:
  0.0 96.1 jit_solution(12686194845268780802)
XLA Ops:
  0.6 93.8 %shard_map.176 = (bf16[128,2048]{1,0:T(8,128)(2,1)S(1)}, bf16[192,2048]{1,0:T(8,128)(2,1)S(1)}) custom-call(bf16[512,256]{1,0:T(8,128)(2,1)} %q_ref.1, bf16[512,256]{1,0:T(8,128)(2,1)} %k_ref.1, bf16[512,256]{1,0:T(8,128)(2,1)} %v_ref.1, f32[1,512]{1,0:T(1,128)} %ig_ref.1, f32[1,512]{1,0:T(1,128)} %fg_ref.1, f32[1,512]{1,0:T(1,128)} %fb_ref.1, ...), custom_call_target="tpu_custom_call" | custom-call | tf_op jit(solution)/shard_map/pallas_call | solution.py:1080
  94.4 0.8 copy.21
  95.2 0.9 copy.22

commit v4 on v3

--- a/solution.py
+++ b/solution.py
@@ -825,7 +825,7 @@
                 for c in group(g):
                     down(s, 1, side, c, weight)
 
-                if g < wc - 1:
+                if g < wc - 2:
                     near_send(s, g)
 
             return carry
@@ -930,13 +930,15 @@
         at(11, hop, i)
     spread(11, 11, near_forward, chunks=range(lead, nc))
     at(9, near_hidden)
+    for g in range(wc - 2):
+        plan[2 * wc + 2 + g].append((near_down, (g,)))
     for g in range(wc - 1):
-        plan[2 * wc + 2 + g].append((near_down, (g,)))
-        at(11, far_step, g)
+        plan[pieces - 3 + g].append((far_step, (g,)))
     last = pieces + 1
-    plan[last - 1] += [(far_step, (wc - 1,)), (far_hidden, ())]
-    plan[last - 1] += [(far_down, (g,)) for g in range(wc // 2)]
-    plan[last] += [(far_down, (g,)) for g in range(wc // 2, wc - 1)]
+    plan[last - 2] += [(far_step, (wc - 1,)), (far_hidden, ())]
+    plan[last - 2] += [(far_down, (g,)) for g in range(wc - 2)]
+    plan[last - 1] += [(near_down, (wc - 2,))]
+    plan[last] += [(far_down, (wc - 2,))]
     plan[last] += [(near_down, (wc - 1,)), (far_down, (wc - 1,)), (hop, (groups - 1,))]
 
     for j in range(pieces + 2):
@@ -960,7 +962,8 @@
         further(d)
 
     for s in (z - 1, z + 1):
-        near_send(s, wc - 1)
+        for g in (wc - 2, wc - 1):
+            near_send(s, g)
 
     def last_turn(g):
         return max(turns.index(t) for t in (g, groups - 1 - g) if t)

time: 96.3 us -> 94.1 us (0.977)
  Pallas kernels: 93.8 us -> 91.6 us
    pallas_call x1, Pallas kernels: 93.8 us -> 91.6 us  [shards(): pl.pallas_call(functools.partial(plane_kernel, n, nt, cap, nc, wc), out_s...]
where the time goes in v4:
time: 94.1 us; the launch traced here: 94 us
  Pallas kernels  91.6 us (97%)
  local copies, waits for them, and re-layouts  1.67 us (2%)
    pallas_call x1, Pallas kernels, shards(): pl.pallas_call(functools.partial(plane_kernel, n, nt, cap, nc, wc), out_s...  91.6 us

profile of v4, /device:TPU:9, one launch (start us, length us, event | category | flops | bytes accessed | tf_op | source)
XLA Modules:
  0.0 94.0 jit_solution(16260541789587422810)
XLA Ops:
  0.6 91.6 %shard_map.176 = (bf16[128,2048]{1,0:T(8,128)(2,1)S(1)}, bf16[192,2048]{1,0:T(8,128)(2,1)S(1)}) custom-call(bf16[512,256]{1,0:T(8,128)(2,1)} %q_ref.1, bf16[512,256]{1,0:T(8,128)(2,1)} %k_ref.1, bf16[512,256]{1,0:T(8,128)(2,1)} %v_ref.1, f32[1,512]{1,0:T(1,128)} %ig_ref.1, f32[1,512]{1,0:T(1,128)} %fg_ref.1, f32[1,512]{1,0:T(1,128)} %fb_ref.1, ...), custom_call_target="tpu_custom_call" | custom-call | tf_op jit(solution)/shard_map/pallas_call | solution.py:1083
  92.3 0.8 copy.21
  93.1 0.9 copy.22
